TPU v7x, 32 devices: a whole 2x2x4 slice. The times are simulated.
32 devices in a mesh: rep: 2 (over core), fs: 8 (over z, y), tp: 2 (over x).
Axes of the slice: x: 2, y: 2, z: 4, core: 2. Of those that a mesh axis runs over, the one named last changes fastest.
Arguments:
- tokens: bfloat16 [8192, 2048], P(('rep', 'fs')), may hold values from -6 to 6
- recurrence_branch_weight: bfloat16 [2048, 2048], P('fs', 'tp'), may hold values from -0.125 to 0.125
- gate_branch_weight: bfloat16 [2048, 2048], P('fs', 'tp'), may hold values from -0.125 to 0.125
- convolution_kernel: bfloat16 [4, 2048], P(None, 'tp'), may hold values from -3 to 3
- recurrence_gate_blockwise: bfloat16 [8, 256, 256], P('tp'), may hold values from -0.375 to 0.375
- input_gate_blockwise: bfloat16 [8, 256, 256], P('tp'), may hold values from -0.375 to 0.375
- channel_decay_param: float32 [2048], P('tp')
- token_decay_shift: float32 [8192, 2048], P(('rep', 'fs'), 'tp'), may hold values from -1 to 0
- recurrence_output_weight: bfloat16 [2048, 2048], P('tp', 'fs'), may hold values from -0.5 to 0.5
- first_norm_gain: float32 [2048], replicated, may hold values from 0.1 to 1.9
- feedforward_gate_weight: bfloat16 [2048, 5120], P('fs', 'tp'), may hold values from -0.125 to 0.125
- feedforward_up_weight: bfloat16 [2048, 5120], P('fs', 'tp'), may hold values from -0.125 to 0.125
- feedforward_down_weight: bfloat16 [5120, 2048], P('tp', 'fs'), may hold values from -0.15625 to 0.15625
- second_norm_gain: float32 [2048], replicated, may hold values from 0.1 to 1.9
Outputs:
- layer_out: bfloat16 [8192, 2048], P(('rep', 'fs', 'tp'))
All inputs are finite; a program needn't handle non-finite values.
Results may differ from a plain program's by a relative error of at most 0.02.
Values may be sent and summed in bfloat16 or wider, within the bound.
A program may use at most 128 MiB of HBM per device.

v0:
```python
import functools

import jax
import jax.numpy as jnp
from jax import lax
from jax.experimental import pallas as pl
from jax.experimental.pallas import tpu as pltpu
from jax.sharding import PartitionSpec as P

residual_scale = 1.4142135623730951

VMEM_BYTES = 60 * 1024 * 1024
LAYER_VMEM_BYTES = 67043328
MESH = pl.DeviceIdType.MESH


def layer_norm(values, gain):
    center = values - jnp.mean(values, axis=-1, keepdims=True)
    variance = jnp.mean(center * center, axis=-1, keepdims=True)
    return center * lax.rsqrt(variance + 1e-05) * gain


def scalars(owners, swapped):
    return jnp.stack([jnp.asarray(v, jnp.int32) for v in [swapped, *owners]])


def split_product(meta, left_ref, part_refs):
    total = None
    for at, part in enumerate(part_refs):
        depth = part.shape[0]
        columns = pl.ds(pl.multiple_of(meta[1 + at] * depth, depth), depth)
        term = jnp.dot(left_ref[:, columns], part[...], preferred_element_type=jnp.float32)
        total = term if total is None else total + term
    return total


def shifted(values, step, fill):
    rows = lax.broadcasted_iota(jnp.int32, values.shape, 0)
    return jnp.where(rows < step, fill, pltpu.roll(values, step, 0))


def sigmoid(values):
    return 1.0 / (1.0 + jnp.exp(-values))


def recur_core(value_in, gate_in, taps, rate_block, inlet_block, plus, shift):
    value_in = value_in.astype(jnp.bfloat16).astype(jnp.float32)
    gate_in = gate_in.astype(jnp.bfloat16).astype(jnp.float32)
    taps = taps.astype(jnp.float32)
    depth = taps.shape[0]
    conv = None
    for tap in range(depth):
        lag = depth - 1 - tap
        moved = value_in if lag == 0 else shifted(value_in, lag, 0.0)
        term = moved * taps[tap : tap + 1, :]
        conv = term if conv is None else conv + term
    conv = conv.astype(jnp.bfloat16)
    rate = sigmoid(jnp.dot(conv, rate_block, preferred_element_type=jnp.float32))
    inlet = sigmoid(jnp.dot(conv, inlet_block, preferred_element_type=jnp.float32))
    log_decay = -8.0 * rate * plus + shift
    decay = jnp.exp(log_decay)
    twice = 2.0 * log_decay
    series = jnp.ones_like(twice)
    for order in range(8, 1, -1):
        series = 1.0 + twice * series * (1.0 / order)
    lost = jnp.where(twice > -0.3, -twice * series, 1.0 - jnp.exp(twice))
    state = jnp.sqrt(lost) * inlet * conv.astype(jnp.float32)
    step = 1
    while step < state.shape[0]:
        state = state + decay * shifted(state, step, 0.0)
        if 2 * step < state.shape[0]:
            decay = decay * shifted(decay, step, 1.0)
        step *= 2
    gelu = 0.5 * gate_in * (
        1.0 + jnp.tanh(0.7978845608028654 * (gate_in + 0.044715 * gate_in * gate_in * gate_in))
    )
    return (state * gelu).astype(jnp.bfloat16)


LINE, OTHER, SIDE, CORE = 0, 1, 2, 3


def layer_kernel(
    tok_hbm,
    in_hbm,
    gate_hbm,
    taps_ref,
    rate_ref,
    inlet_ref,
    plus_ref,
    shift_hbm,
    out_hbm,
    first_gain_ref,
    ffgate_hbm,
    ffup_hbm,
    down_hbm,
    second_gain_ref,
    out_ref,
    buf_a,
    buf_b,
    buf_c,
    buf_d,
    tok,
    shift,
    branch,
    terms,
    came,
    normed,
    hidden,
    load_sem,
    send_sem,
    recv_sem,
    terms_send,
    terms_recv,
    norm_send,
    norm_recv,
):
    core, fs, tp = lax.axis_index("rep"), lax.axis_index("fs"), lax.axis_index("tp")
    z, y = fs // 2, fs % 2
    zs = [z, z + 1 - 2 * (z % 2), 2 - z // 2, 3 - 3 * (z // 2)]
    middle = z * (3 - z) == 2
    first_core, second_core = core == 0, core == 1
    second_middle = jnp.logical_and(second_core, middle)
    first_or_end = jnp.logical_or(first_core, jnp.logical_not(middle))
    far = 3 - z
    own_at = [k * 2 + y for k in zs]
    side_at = [k * 2 + 1 - y for k in zs]
    me = own_at[0]
    targets = {
        LINE: (core, own_at[1], tp),
        OTHER: (core, far * 2 + y, tp),
        SIDE: (core, side_at[0], tp),
        CORE: (1 - core, me, tp),
    }
    across = (core, me, 1 - tp)
    width = in_hbm.shape[0]
    ff_half = buf_c.shape[3]
    columns = buf_b.shape[2]
    mix_depth, down_depth = buf_b.shape[1], buf_d.shape[1]
    share = out_ref.shape[0]
    tile = min(256, ff_half)
    own_row = pl.multiple_of(tp * share, share)
    sent = []

    def piece(pack, at, half):
        if pack == 0:
            return buf_a.at[half, pl.ds(pl.multiple_of(at * width, width), width), :]
        if pack == 1:
            rows = mix_depth // 2
            return buf_b.at[at, pl.ds(pl.multiple_of(half * rows, rows), rows), :]
        if pack < 4:
            return buf_c.at[pack - 2, half, pl.ds(pl.multiple_of(at * width, width), width), :]
        rows = down_depth // 4
        return buf_d.at[at, pl.ds(pl.multiple_of((half * 2 + pack - 4) * rows, rows), rows), :]

    def copy(pack, at, way, half=core):
        return pltpu.make_async_remote_copy(
            src_ref=piece(pack, at, half),
            dst_ref=piece(pack, at, half),
            send_sem=send_sem.at[pack, at, way],
            recv_sem=recv_sem.at[pack, half, at],
            device_id=targets[way],
            device_id_type=MESH,
        )

    def under(condition, action):
        if condition is None:
            action()
        else:
            pl.when(condition)(action)

    def send(pack, at, way, condition=None):
        sent.append((pack, at, way, condition))
        under(condition, lambda: copy(pack, at, way).start())

    def arrived(pack, at):
        copy(pack, at, CORE).wait_recv()

    def handed(pack, at):
        copy(pack, at, CORE, 1 - core).wait_recv()

    def send_own(pack):
        send(pack, me, LINE)
        send(pack, me, OTHER, middle)
        send(pack, me, SIDE)

    def from_side(pack):
        at = side_at[0]
        arrived(pack, at)
        send(pack, at, LINE, second_core)
        send(pack, at, OTHER, second_middle)
        send(pack, at, CORE)

    def from_line(pack, k):
        at = own_at[k]
        arrived(pack, at)
        send(pack, at, OTHER if k == 1 else LINE, middle)
        if k == 3:
            send(pack, at, SIDE)
        elif k == 2:
            send(pack, at, SIDE, first_or_end)
        else:
            send(pack, at, SIDE, first_core)
        send(pack, at, CORE)

    def from_far_side(pack, k):
        at = side_at[k]
        arrived(pack, at)
        send(pack, at, CORE)

    def events(pack):
        return [
            lambda: from_side(pack),
            lambda: from_line(pack, 1),
            lambda: from_line(pack, 2),
            lambda: from_far_side(pack, 1),
            lambda: from_line(pack, 3),
            lambda: from_far_side(pack, 2),
            lambda: from_far_side(pack, 3),
        ]

    order = [me, side_at[0], own_at[1], own_at[2], side_at[1], own_at[3], side_at[2], side_at[3]]

    def all_handed(pack):
        for at in order[1:]:
            handed(pack, at)

    def run(actions):
        for action in actions:
            action()

    def at_step(step, plan):
        for when, actions in enumerate(plan):
            if actions:
                pl.when(step == when)(functools.partial(run, actions))

    c_cols = lambda half: pl.ds(half * ff_half, ff_half)
    loads = {
        "a0": (in_hbm, piece(0, me, 0)),
        "a1": (gate_hbm, piece(0, me, 1)),
        "b": (out_hbm, buf_b.at[me]),
        "tok": (tok_hbm, tok),
        "c0": (ffgate_hbm.at[:, c_cols(0)], piece(2, me, 0)),
        "c1": (ffup_hbm.at[:, c_cols(0)], piece(2, me, 1)),
        "c2": (ffgate_hbm.at[:, c_cols(1)], piece(3, me, 0)),
        "c3": (ffup_hbm.at[:, c_cols(1)], piece(3, me, 1)),
        "d": (down_hbm, buf_d.at[me]),
        "shift": (shift_hbm, shift),
    }
    loads = {
        name: pltpu.make_async_copy(source, target, load_sem.at[at])
        for at, (name, (source, target)) in enumerate(loads.items())
    }
    for load in loads.values():
        load.start()

    barrier = pltpu.get_barrier_semaphore()
    for target in [targets[LINE], targets[SIDE], targets[CORE], across]:
        pl.semaphore_signal(barrier, inc=1, device_id=target, device_id_type=MESH)

    @pl.when(middle)
    def _():
        pl.semaphore_signal(barrier, inc=1, device_id=targets[OTHER], device_id_type=MESH)

    pl.semaphore_wait(barrier, 4 + z * (3 - z) // 2)

    loads["a0"].wait()
    loads["a1"].wait()
    send_own(0)
    loads["b"].wait()
    send_own(1)
    run(events(0)[:5])
    for name in ("c0", "c1"):
        loads[name].wait()
    send_own(2)
    run(events(0)[5:])
    all_handed(0)
    loads["tok"].wait()
    loads["shift"].wait()

    block = rate_ref.shape[1]

    def recur_step(i, plan):
        cols = pl.ds(pl.multiple_of(i * block, block), block)
        value_in = jnp.dot(tok[...], buf_a[0, :, cols], preferred_element_type=jnp.float32)
        gate_in = jnp.dot(tok[...], buf_a[1, :, cols], preferred_element_type=jnp.float32)
        branch[:, cols] = recur_core(
            value_in, gate_in, taps_ref[:, cols], rate_ref[i], inlet_ref[i], plus_ref[:, cols], shift[:, cols]
        )
        at_step(i, plan)

    ev = events(1)
    plan = [ev[:2], ev[2:4], ev[4:5], ev[5:]]
    lax.fori_loop(0, rate_ref.shape[0], lambda i, _: recur_step(i, plan), None)
    for name in ("c2", "c3"):
        loads[name].wait()
    send_own(3)
    all_handed(1)

    def terms_copy(phase, at):
        return pltpu.make_async_remote_copy(
            src_ref=terms.at[1 - tp, at],
            dst_ref=came.at[phase, at],
            send_sem=terms_send.at[phase, at],
            recv_sem=terms_recv.at[phase, at],
            device_id=across,
            device_id_type=MESH,
        )

    def keep(product, at):
        product = product.astype(jnp.bfloat16)
        for row in range(2):
            terms[row, at] = product[row * share : (row + 1) * share]

    parts = buf_b.shape[0]

    def mix_step(s, _):
        keep(jnp.dot(branch[...], buf_b[s], preferred_element_type=jnp.float32), s)
        pl.when(s > 0)(lambda: terms_copy(0, s - 1).start())

    lax.fori_loop(0, parts, mix_step, None)
    ev = events(2)
    run(ev[:1])
    terms_copy(0, parts - 1).start()
    run(ev[1:2])
    for s in range(parts):
        terms_copy(0, s).wait_recv()

    rows = 64

    def norm_rows(i, phase, residual, gain_ref):
        piece_rows = pl.ds(pl.multiple_of(i * rows, rows), rows)
        value = jnp.concatenate(
            [
                terms[tp, s, piece_rows, :].astype(jnp.float32) + came[phase, s, piece_rows, :].astype(jnp.float32)
                for s in range(parts)
            ],
            axis=1,
        )
        return layer_norm(residual_scale * residual.astype(jnp.float32) + value, gain_ref[...]).astype(jnp.bfloat16)

    def own_rows(i):
        return pl.ds(pl.multiple_of(own_row + i * rows, rows), rows)

    def norm_copy(i):
        return pltpu.make_async_remote_copy(
            src_ref=normed.at[own_rows(i), :],
            dst_ref=normed.at[own_rows(i), :],
            send_sem=norm_send.at[i],
            recv_sem=norm_recv.at[i],
            device_id=across,
            device_id_type=MESH,
        )

    def first_norm(i, _):
        normed[own_rows(i), :] = norm_rows(i, 0, tok[own_rows(i), :], first_gain_ref)
        pl.when(i > 0)(lambda: norm_copy(i - 1).start())

    tiles = share // rows
    lax.fori_loop(0, tiles, first_norm, None)
    run(ev[2:3])
    norm_copy(tiles - 1).start()
    run(ev[3:5])
    loads["d"].wait()
    send_own(4)
    run(ev[5:])
    for i in range(tiles):
        norm_copy(i).wait_recv()
    all_handed(2)

    def hidden_step(j, half, plan):
        cols = pl.ds(pl.multiple_of(j * tile, tile), tile)
        gate = jnp.dot(normed[...], buf_c[half, 0, :, cols], preferred_element_type=jnp.float32)
        upward = jnp.dot(normed[...], buf_c[half, 1, :, cols], preferred_element_type=jnp.float32)
        to = pl.ds(pl.multiple_of(half * ff_half + j * tile, tile), tile)
        hidden[:, to] = (gate * sigmoid(gate) * upward).astype(jnp.bfloat16)
        at_step(j, plan)

    steps = ff_half // tile
    ev = events(3)
    plan = [ev[:2], ev[2:3], ev[3:4], ev[4:5], []]
    lax.fori_loop(0, steps, lambda j, _: hidden_step(j, 0, plan), None)
    send_own(5)
    run(ev[5:])
    all_handed(3)
    ev = events(4)
    plan = [ev[:2], ev[2:3], ev[3:5], ev[5:6], []]
    lax.fori_loop(0, steps, lambda j, _: hidden_step(j, 1, plan), None)
    run(ev[6:])

    for s in range(parts):
        terms_copy(0, s).wait_send()

    ev = events(5)

    def pick(j):
        at = order[0]
        for turn in range(1, parts):
            at = jnp.where(j == turn, order[turn], at)
        return at

    def down_step(j, _):
        at_step(j, [[]] + [[e] for e in ev])
        at = pick(j)
        @pl.when(j > 0)
        def _():
            handed(4, at)
            handed(5, at)
        keep(jnp.dot(hidden[...], buf_d[at], preferred_element_type=jnp.float32), at)
        pl.when(j > 0)(lambda: terms_copy(1, pick(j - 1)).start())

    lax.fori_loop(0, parts, down_step, None)
    for pack, at, way, condition in sent:
        under(condition, lambda: copy(pack, at, way).wait_send())
    terms_copy(1, order[-1]).start()
    for s in order:
        terms_copy(1, s).wait_recv()

    def second_norm(i, _):
        here = pl.ds(pl.multiple_of(i * rows, rows), rows)
        out_ref[here, :] = norm_rows(i, 1, normed[own_rows(i), :], second_gain_ref)

    lax.fori_loop(0, tiles, second_norm, None)
    for i in range(tiles):
        norm_copy(i).wait_send()
    for s in range(parts):
        terms_copy(1, s).wait_send()


def whole_layer(
    tokens,
    recurrence_branch_weight,
    gate_branch_weight,
    convolution_kernel,
    recurrence_gate_blockwise,
    input_gate_blockwise,
    channel_decay_param,
    token_decay_shift,
    recurrence_output_weight,
    first_norm_gain,
    feedforward_gate_weight,
    feedforward_up_weight,
    feedforward_down_weight,
    second_norm_gain,
):
    length, model = tokens.shape
    parts = lax.axis_size("fs")
    share = length // lax.axis_size("tp")
    depth, channels = recurrence_branch_weight.shape
    units = feedforward_gate_weight.shape[1]
    columns = recurrence_output_weight.shape[1]
    hbm = pl.BlockSpec(memory_space=pl.ANY)
    vmem = pl.BlockSpec(memory_space=pltpu.VMEM)
    half = jnp.bfloat16
    return pl.pallas_call(
        layer_kernel,
        in_specs=[hbm, hbm, hbm, vmem, vmem, vmem, vmem, hbm, hbm, vmem, hbm, hbm, hbm, vmem],
        out_specs=vmem,
        out_shape=jax.ShapeDtypeStruct((share, model), half),
        scratch_shapes=[
            pltpu.VMEM((2, depth * parts, channels), half),
            pltpu.VMEM((parts, channels, columns), half),
            pltpu.VMEM((2, 2, depth * parts, units // 2), half),
            pltpu.VMEM((parts, units, columns), half),
            pltpu.VMEM((length, model), half),
            pltpu.VMEM((length, channels), jnp.float32),
            pltpu.VMEM((length, channels), half),
            pltpu.VMEM((2, parts, share, columns), half),
            pltpu.VMEM((2, parts, share, columns), half),
            pltpu.VMEM((length, model), half),
            pltpu.VMEM((length, units), half),
            pltpu.SemaphoreType.DMA((10,)),
            pltpu.SemaphoreType.DMA((6, parts, 4)),
            pltpu.SemaphoreType.DMA((6, 2, parts)),
            pltpu.SemaphoreType.DMA((2, parts)),
            pltpu.SemaphoreType.DMA((2, parts)),
            pltpu.SemaphoreType.DMA((share // 64,)),
            pltpu.SemaphoreType.DMA((share // 64,)),
        ],
        cost_estimate=pl.CostEstimate(
            flops=2 * length * model * (2 * channels + 2 * units) + 2 * length * model * (channels + units),
            bytes_accessed=2 * model * (3 * channels + 3 * units),
            transcendentals=0,
        ),
        compiler_params=pltpu.CompilerParams(
            vmem_limit_bytes=LAYER_VMEM_BYTES, collective_id=0, has_side_effects=True
        ),
    )(
        tokens,
        recurrence_branch_weight,
        gate_branch_weight,
        convolution_kernel,
        recurrence_gate_blockwise,
        input_gate_blockwise,
        jax.nn.softplus(-channel_decay_param)[None, :],
        token_decay_shift,
        recurrence_output_weight,
        first_norm_gain[None, :],
        feedforward_gate_weight,
        feedforward_up_weight,
        feedforward_down_weight,
        second_norm_gain[None, :],
    )


def recurrence_kernel(count, meta, x_ref, taps_ref, rate_ref, inlet_ref, plus_ref, shift_ref, *refs):
    mine, other, out_ref = refs[:count], refs[count : 2 * count], refs[-1]
    first = split_product(meta, x_ref, mine)
    second = split_product(meta, x_ref, other)
    out_ref[...] = recur_core(
        first, second, taps_ref[...], rate_ref[0], inlet_ref[0], plus_ref[...], shift_ref[...]
    )


def recurrence(tokens, mine, other, meta, taps, rate_blocks, inlet_blocks, plus, shift):
    length, width = tokens.shape
    block = rate_blocks.shape[1]
    blocks = rate_blocks.shape[0]
    parts = [pl.BlockSpec((p.shape[0], block), lambda i: (0, i)) for p in [*mine, *other]]
    column = lambda rows: pl.BlockSpec((rows, block), lambda i: (0, i))
    square = pl.BlockSpec((1, block, block), lambda i: (i, 0, 0))
    return pl.pallas_call(
        functools.partial(recurrence_kernel, len(mine)),
        grid=(blocks,),
        in_specs=[
            pl.BlockSpec(memory_space=pltpu.SMEM),
            pl.BlockSpec((length, width), lambda i: (0, 0)),
            column(taps.shape[0]),
            square,
            square,
            column(1),
            column(length),
            *parts,
        ],
        out_specs=column(length),
        out_shape=jax.ShapeDtypeStruct((length, block * blocks), jnp.bfloat16),
        cost_estimate=pl.CostEstimate(
            flops=4 * length * width * block * blocks,
            bytes_accessed=4 * width * block * blocks + 8 * length * block * blocks,
            transcendentals=0,
        ),
        compiler_params=pltpu.CompilerParams(vmem_limit_bytes=VMEM_BYTES),
    )(meta, tokens, taps, rate_blocks, inlet_blocks, plus, shift, *mine, *other)


def hidden_kernel(count, meta, x_ref, *refs):
    mine, other, out_ref = refs[:count], refs[count : 2 * count], refs[-1]
    first = split_product(meta, x_ref, mine)
    second = split_product(meta, x_ref, other)
    swapped = meta[0] == 1
    gate = jnp.where(swapped, second, first)
    upward = jnp.where(swapped, first, second)
    out_ref[...] = (gate * sigmoid(gate) * upward).astype(jnp.bfloat16)


def hidden_units(normed, mine, other, meta):
    length, width = normed.shape
    units = mine[0].shape[1]
    tile = next(t for t in (512, 640, 256, 128, units) if units % t == 0)
    return pl.pallas_call(
        functools.partial(hidden_kernel, len(mine)),
        grid=(units // tile,),
        in_specs=[
            pl.BlockSpec(memory_space=pltpu.SMEM),
            pl.BlockSpec((length, width), lambda i: (0, 0)),
            *[pl.BlockSpec((p.shape[0], tile), lambda i: (0, i)) for p in [*mine, *other]],
        ],
        out_specs=pl.BlockSpec((length, tile), lambda i: (0, i)),
        out_shape=jax.ShapeDtypeStruct((length, units), jnp.bfloat16),
        cost_estimate=pl.CostEstimate(
            flops=4 * length * width * units, bytes_accessed=4 * width * units, transcendentals=0
        ),
        compiler_params=pltpu.CompilerParams(vmem_limit_bytes=VMEM_BYTES),
    )(meta, normed, *mine, *other)


def outward_kernel(count, meta, left_ref, *refs):
    mine, other, out_ref = refs[:count], refs[count : 2 * count], refs[-1]
    half = mine[0].shape[0]
    near = pl.ds(pl.multiple_of(meta[0] * half, 128), half)
    far = pl.ds(pl.multiple_of((1 - meta[0]) * half, 128), half)
    start = 0
    for at in range(count):
        total = jnp.dot(left_ref[:, near], mine[at][...], preferred_element_type=jnp.float32)
        total += jnp.dot(left_ref[:, far], other[at][...], preferred_element_type=jnp.float32)
        columns = mine[at].shape[1]
        out_ref[:, start : start + columns] = total.astype(jnp.bfloat16)
        start += columns


def outward(left, mine, other, meta):
    length, depth = left.shape
    width = sum(p.shape[1] for p in mine)
    rows = min(length, 256)
    whole = [pl.BlockSpec(p.shape, lambda i: (0, 0)) for p in [*mine, *other]]
    return pl.pallas_call(
        functools.partial(outward_kernel, len(mine)),
        grid=(length // rows,),
        in_specs=[
            pl.BlockSpec(memory_space=pltpu.SMEM),
            pl.BlockSpec((rows, depth), lambda i: (i, 0)),
            *whole,
        ],
        out_specs=pl.BlockSpec((rows, width), lambda i: (i, 0)),
        out_shape=jax.ShapeDtypeStruct((length, width), jnp.bfloat16),
        cost_estimate=pl.CostEstimate(
            flops=2 * length * width * depth, bytes_accessed=2 * width * depth, transcendentals=0
        ),
        compiler_params=pltpu.CompilerParams(vmem_limit_bytes=VMEM_BYTES),
    )(meta, left, *mine, *other)


def gathered_layer(
    tokens,
    recurrence_branch_weight,
    gate_branch_weight,
    convolution_kernel,
    recurrence_gate_blockwise,
    input_gate_blockwise,
    channel_decay_param,
    token_decay_shift,
    recurrence_output_weight,
    first_norm_gain,
    feedforward_gate_weight,
    feedforward_up_weight,
    feedforward_down_weight,
    second_norm_gain,
):
    share = tokens.shape[0] // lax.axis_size("tp")
    offset = lax.axis_index("tp") * share
    rows_of = lambda weight: [lax.all_gather(weight, "fs", axis=0, tiled=True)]

    def halves_of(weight):
        half = weight.shape[0] // 2
        return [[lax.all_gather(part, "fs", axis=1, tiled=True)] for part in (weight[:half], weight[half:])]

    meta = scalars([jnp.int32(0)], jnp.int32(0))
    branch = recurrence(
        tokens,
        rows_of(recurrence_branch_weight),
        rows_of(gate_branch_weight),
        meta,
        convolution_kernel,
        recurrence_gate_blockwise,
        input_gate_blockwise,
        jax.nn.softplus(-channel_decay_param)[None, :],
        token_decay_shift,
    )

    def grouped(left, weight):
        terms = outward(left, *halves_of(weight), meta)
        return lax.psum_scatter(terms, "tp", scatter_dimension=0, tiled=True).astype(jnp.float32)

    mix = grouped(branch, recurrence_output_weight)
    own_tokens = lax.dynamic_slice_in_dim(tokens, offset, share, 0)
    normed = layer_norm(
        residual_scale * own_tokens.astype(jnp.float32) + mix, first_norm_gain
    ).astype(jnp.bfloat16)
    rows = lax.all_gather(normed, "tp", axis=0, tiled=True)
    hidden = hidden_units(rows, rows_of(feedforward_gate_weight), rows_of(feedforward_up_weight), meta)
    ffn = grouped(hidden, feedforward_down_weight)
    return layer_norm(residual_scale * normed.astype(jnp.float32) + ffn, second_norm_gain).astype(
        jnp.bfloat16
    )


def solution(mesh):
    sizes = mesh.shape
    one_kernel = sizes["rep"] == 2 and sizes["tp"] == 2 and sizes["fs"] == 8
    return jax.shard_map(
        whole_layer if one_kernel else gathered_layer,
        mesh=mesh,
        in_specs=(
            P(("rep", "fs"), None),
            P("fs", "tp"),
            P("fs", "tp"),
            P(None, "tp"),
            P("tp", None, None),
            P("tp", None, None),
            P("tp"),
            P(("rep", "fs"), "tp"),
            P("tp", "fs"),
            P(),
            P("fs", "tp"),
            P("fs", "tp"),
            P("tp", "fs"),
            P(),
        ),
        out_specs=P(("rep", "fs", "tp"), None),
        check_vma=False,
    )
```

profile of v0, /device:TPU:0, one launch (start us, length us, event | category | flops | bytes accessed | tf_op | source)
XLA Modules:
  0.0 263.1 jit_solution(4511985671030989523)
XLA Ops:
  0.0 1.3 compare_select_fusion
  1.3 259.5 %shard_map.136 = bf16[256,2048]{1,0:T(8,128)(2,1)} custom-call(bf16[512,2048]{1,0:T(8,128)(2,1)} %tok_hbm.1, bf16[256,1024]{1,0:T(8,128)(2,1)} %in_hbm.1, bf16[256,1024]{1,0:T(8,128)(2,1)} %gate_hbm.1, bf16[4,1024]{1,0:T(4,128)(2,1)} %taps_ref.1, bf16[4,256,256]{2,1,0:T(8,128)(2,1)} %rate_ref.1, bf16[4,256,256]{2,1,0:T(8,128)(2,1)} %inlet_ref.1, ...), custom_call_target="tpu_custom_call" | custom-call | flops 22548578304 | bytes 44040192 | tf_op jit(solution)/shard_map/pallas_call | solution.py:455
  260.8 2.3 copy.16
where the time goes:
time: 264 us; the launch traced here: 263 us
  Pallas kernels  260 us (98%)
    pallas_call x1, Pallas kernels, whole_layer(): pl.pallas_call(layer_kernel, in_specs=[hbm, hbm, hbm, vmem, vmem, vmem, v...  260 us

commit v1 on v0

--- a/solution.py
+++ b/solution.py
@@ -78,6 +78,40 @@
 
 
 LINE, OTHER, SIDE, CORE = 0, 1, 2, 3
+OWN, OWN_SIDE, FROM_SIDE, FROM_LINE, ON_SIDE, FROM_FAR_SIDE = range(6)
+PACKS = ((0, 0, 1), (1, 0, 1), (2, 0, 1), (3, 0, 1), (4, 0, 2), (4, 1, 2))
+PLANS = (
+    (
+        (100, 110, 0, 10, 401, 130, 402, 403),
+        (503, 412, 303, 200, 312, 210, 20, 501, 413, 30, 150, 502, 431, 411, 313, 302, 421, 120, 512),
+        (50, 311, 511, 513, 301), (432,), (), (), (331, 322), (), (321,), (422,), (220, 40, 451), (230, 423), (),
+        (521,), (433, 341), (523,), (351, 522, 333, 140), (441,), (323, 533, 532), (), (), (332,), (), (531, 442),
+        (), (), (250, 452), (342,), (352,), (240, 443, 551, 541), (343,), (543,), (353, 453, 552), (542,), (553,),
+        (),
+    ),
+    (
+
+        (130, 100, 0, 10, 301, 20, 200, 403, 110, 401, 503, 402, 302, 421, 120, 412, 303, 312, 501, 150, 502, 210, 411),
+        (413,), (313, 50), (311, 512, 40, 513, 511, 432), (), (), (), (), (322, 30), (140,), (331,), (422,),
+        (451, 230), (332,), (), (), (), (220, 321, 323, 522, 423, 521), (531,), (351, 441), (532, 431),
+        (523, 333, 433, 533), (442, 250), (), (240,), (), (342, 452), (), (), (352,), (), (551, 552),
+        (341, 443, 343, 541), (353, 542, 453, 543), (), (553,),
+    ),
+    (
+        (0, 100, 110, 401, 301, 311, 10, 302, 403, 130, 303, 402), (313, 312, 501, 210, 503, 30, 150),
+        (200, 412, 20, 411, 502, 50), (120, 413), (512, 513, 511), (432,), (332,), (), (422,), (322,), (331,),
+        (140, 321), (451,), (230, 323, 431, 423), (), (), (351,), (341, 421),
+        (523, 522, 220, 333, 441, 531, 40, 250, 532, 521), (433,), (), (), (533,), (342,), (352, 452), (),
+        (343, 240, 442), (), (443, 551), (), (543, 552, 541), (542, 353, 453), (553,), (), (), (),
+    ),
+    (
+        (100, 401, 0, 10, 110, 302, 311, 402, 312, 301, 303, 403, 501, 413, 200, 20, 30, 503, 502, 150), (), (411,),
+        (), (210, 313, 332, 50, 412, 321, 130, 513, 511), (), (120,), (), (512,), (422, 322, 40, 331), (323,),
+        (230, 451, 140, 423), (), (), (), (220,), (521,), (421, 432, 433, 523), (522,), (441, 531), (), (333,),
+        (351, 342, 532), (), (250, 352), (533,), (), (341, 431, 443, 442), (551, 240), (), (343, 552), (), (),
+        (543, 353, 453, 542), (), (452, 541, 553),
+    ),
+)
 
 
 def layer_kernel(
@@ -85,9 +119,9 @@
     in_hbm,
     gate_hbm,
     taps_ref,
-    rate_ref,
-    inlet_ref,
-    plus_ref,
+    rate_hbm,
+    inlet_hbm,
+    param_ref,
     shift_hbm,
     out_hbm,
     first_gain_ref,
@@ -101,6 +135,8 @@
     buf_c,
     buf_d,
     tok,
+    rate_blocks,
+    inlet_blocks,
     shift,
     branch,
     terms,
@@ -119,39 +155,42 @@
     z, y = fs // 2, fs % 2
     zs = [z, z + 1 - 2 * (z % 2), 2 - z // 2, 3 - 3 * (z // 2)]
     middle = z * (3 - z) == 2
-    first_core, second_core = core == 0, core == 1
-    second_middle = jnp.logical_and(second_core, middle)
-    first_or_end = jnp.logical_or(first_core, jnp.logical_not(middle))
-    far = 3 - z
-    own_at = [k * 2 + y for k in zs]
-    side_at = [k * 2 + 1 - y for k in zs]
-    me = own_at[0]
+    role = core + z * (3 - z)
+    roles = [role == at for at in range(4)]
+    spots = [[k * 2 + y for k in zs], [k * 2 + 1 - y for k in zs]]
+    me = spots[0][0]
     targets = {
-        LINE: (core, own_at[1], tp),
-        OTHER: (core, far * 2 + y, tp),
-        SIDE: (core, side_at[0], tp),
+        LINE: (core, spots[0][1], tp),
+        OTHER: (core, (3 - z) * 2 + y, tp),
+        SIDE: (core, spots[1][0], tp),
         CORE: (1 - core, me, tp),
     }
     across = (core, me, 1 - tp)
     width = in_hbm.shape[0]
+    parts = buf_b.shape[0]
     ff_half = buf_c.shape[3]
-    columns = buf_b.shape[2]
     mix_depth, down_depth = buf_b.shape[1], buf_d.shape[1]
     share = out_ref.shape[0]
+    block = rate_blocks.shape[1]
+    blocks = rate_blocks.shape[0]
     tile = min(256, ff_half)
+    tiles = ff_half // tile
+    rows = min(64, share)
+    row_tiles = share // rows
     own_row = pl.multiple_of(tp * share, share)
-    sent = []
+
+    def run_of(base, part, count):
+        return pl.ds(pl.multiple_of(base + part * count, count), count)
 
     def piece(pack, at, half):
-        if pack == 0:
-            return buf_a.at[half, pl.ds(pl.multiple_of(at * width, width), width), :]
-        if pack == 1:
-            rows = mix_depth // 2
-            return buf_b.at[at, pl.ds(pl.multiple_of(half * rows, rows), rows), :]
-        if pack < 4:
-            return buf_c.at[pack - 2, half, pl.ds(pl.multiple_of(at * width, width), width), :]
-        rows = down_depth // 4
-        return buf_d.at[at, pl.ds(pl.multiple_of((half * 2 + pack - 4) * rows, rows), rows), :]
+        weight, part, count = PACKS[pack]
+        if weight == 0:
+            return buf_a.at[half, run_of(at * width, part, width // count), :]
+        if weight == 1:
+            return buf_b.at[at, run_of(half * (mix_depth // 2), part, mix_depth // 2 // count), :]
+        if weight < 4:
+            return buf_c.at[weight - 2, half, run_of(at * width, part, width // count), :]
+        return buf_d.at[at, run_of(half * (down_depth // 2), part, down_depth // 2 // count), :]
 
     def copy(pack, at, way, half=core):
         return pltpu.make_async_remote_copy(
@@ -163,97 +202,136 @@
             device_id_type=MESH,
         )
 
-    def under(condition, action):
-        if condition is None:
-            action()
-        else:
-            pl.when(condition)(action)
-
-    def send(pack, at, way, condition=None):
-        sent.append((pack, at, way, condition))
-        under(condition, lambda: copy(pack, at, way).start())
-
-    def arrived(pack, at):
-        copy(pack, at, CORE).wait_recv()
-
-    def handed(pack, at):
-        copy(pack, at, CORE, 1 - core).wait_recv()
-
-    def send_own(pack):
-        send(pack, me, LINE)
-        send(pack, me, OTHER, middle)
-        send(pack, me, SIDE)
-
-    def from_side(pack):
-        at = side_at[0]
-        arrived(pack, at)
-        send(pack, at, LINE, second_core)
-        send(pack, at, OTHER, second_middle)
-        send(pack, at, CORE)
-
-    def from_line(pack, k):
-        at = own_at[k]
-        arrived(pack, at)
-        send(pack, at, OTHER if k == 1 else LINE, middle)
-        if k == 3:
-            send(pack, at, SIDE)
-        elif k == 2:
-            send(pack, at, SIDE, first_or_end)
-        else:
-            send(pack, at, SIDE, first_core)
-        send(pack, at, CORE)
-
-    def from_far_side(pack, k):
-        at = side_at[k]
-        arrived(pack, at)
-        send(pack, at, CORE)
-
-    def events(pack):
-        return [
-            lambda: from_side(pack),
-            lambda: from_line(pack, 1),
-            lambda: from_line(pack, 2),
-            lambda: from_far_side(pack, 1),
-            lambda: from_line(pack, 3),
-            lambda: from_far_side(pack, 2),
-            lambda: from_far_side(pack, 3),
-        ]
-
-    order = [me, side_at[0], own_at[1], own_at[2], side_at[1], own_at[3], side_at[2], side_at[3]]
-
-    def all_handed(pack):
-        for at in order[1:]:
-            handed(pack, at)
-
-    def run(actions):
-        for action in actions:
-            action()
-
-    def at_step(step, plan):
-        for when, actions in enumerate(plan):
-            if actions:
-                pl.when(step == when)(functools.partial(run, actions))
-
     c_cols = lambda half: pl.ds(half * ff_half, ff_half)
-    loads = {
-        "a0": (in_hbm, piece(0, me, 0)),
-        "a1": (gate_hbm, piece(0, me, 1)),
-        "b": (out_hbm, buf_b.at[me]),
-        "tok": (tok_hbm, tok),
-        "c0": (ffgate_hbm.at[:, c_cols(0)], piece(2, me, 0)),
-        "c1": (ffup_hbm.at[:, c_cols(0)], piece(2, me, 1)),
-        "c2": (ffgate_hbm.at[:, c_cols(1)], piece(3, me, 0)),
-        "c3": (ffup_hbm.at[:, c_cols(1)], piece(3, me, 1)),
-        "d": (down_hbm, buf_d.at[me]),
-        "shift": (shift_hbm, shift),
-    }
-    loads = {
-        name: pltpu.make_async_copy(source, target, load_sem.at[at])
-        for at, (name, (source, target)) in enumerate(loads.items())
-    }
-    for load in loads.values():
-        load.start()
-
+    own_rows_of = lambda ref, *at: ref.at[(*at, pl.ds(pl.multiple_of(me * width, width), width), slice(None))]
+    loads = [
+        [(in_hbm, own_rows_of(buf_a, 0)), (gate_hbm, own_rows_of(buf_a, 1))],
+        [(out_hbm, buf_b.at[me])],
+        [(ffgate_hbm.at[:, c_cols(0)], own_rows_of(buf_c, 0, 0)), (ffup_hbm.at[:, c_cols(0)], own_rows_of(buf_c, 0, 1))],
+        [(ffgate_hbm.at[:, c_cols(1)], own_rows_of(buf_c, 1, 0)), (ffup_hbm.at[:, c_cols(1)], own_rows_of(buf_c, 1, 1))],
+        [(down_hbm, buf_d.at[me])],
+        [(tok_hbm, tok), (shift_hbm, shift), (rate_hbm, rate_blocks), (inlet_hbm, inlet_blocks)],
+    ]
+    count = 0
+    for group in loads:
+        for at, (source, target) in enumerate(group):
+            group[at] = pltpu.make_async_copy(source, target, load_sem.at[count])
+            count += 1
+
+    steps = ["recur"] * blocks + ["mix"] * parts + ["terms"] + ["norm"] * row_tiles + ["rows"]
+    steps += ["hidden0"] * tiles + ["hidden1"] * tiles + ["down"] * parts
+    begins = {name: steps.index(name) for name in dict.fromkeys(steps)}
+    turn_of = [(0, 0), (0, 1), (1, 0), (2, 0), (1, 1), (3, 0), (2, 1), (3, 1)]
+    needs = {begins["recur"]: 0, begins["mix"]: 1, begins["hidden0"]: 2, begins["hidden1"]: 3}
+    packs_of = [[p for p, (w, _, _) in enumerate(PACKS) if w == weight] for weight in range(5)]
+
+    def actions(plan, in_middle, second):
+        loaded, waited, sends, gaps = set(), set(), [], []
+
+        def load(weight, out):
+            if weight not in loaded:
+                loaded.add(weight)
+                out.append(("load", weight))
+
+        def arrive(pack, k, side, out):
+            if (k, side) == (0, 0):
+                load(PACKS[pack][0], out)
+            elif (pack, k, side) not in waited:
+                waited.add((pack, k, side))
+                out.append(("arrive", pack, k, side))
+
+        def send(pack, k, side, way, out):
+            arrive(pack, k, side, out)
+            out.append(("send", pack, k, side, way))
+            sends.append((pack, k, side, way, len(gaps)))
+
+        for step, codes in enumerate(plan):
+            out = []
+            for code in codes:
+                kind, pack, k = code // 100, code // 10 % 10, code % 10
+                if kind == OWN:
+                    send(pack, 0, 0, LINE, out)
+                    if in_middle:
+                        send(pack, 0, 0, OTHER, out)
+                elif kind == OWN_SIDE:
+                    send(pack, 0, 0, SIDE, out)
+                elif kind == FROM_SIDE:
+                    arrive(pack, 0, 1, out)
+                    if second:
+                        send(pack, 0, 1, LINE, out)
+                        if in_middle:
+                            send(pack, 0, 1, OTHER, out)
+                    send(pack, 0, 1, CORE, out)
+                elif kind == FROM_LINE:
+                    if in_middle:
+                        send(pack, k, 0, OTHER if k == 1 else LINE, out)
+                    send(pack, k, 0, CORE, out)
+                elif kind == ON_SIDE:
+                    if k == 3 or not second or (k == 2 and not in_middle):
+                        send(pack, k, 0, SIDE, out)
+                else:
+                    send(pack, k, 1, CORE, out)
+            if step in needs:
+                weight = needs[step]
+                load(weight, out)
+                if step == 0:
+                    load(5, out)
+                for pack in packs_of[weight]:
+                    for turn in turn_of[1:]:
+                        arrive(pack, *turn, out)
+                        out.append(("handed", pack, *turn))
+            if begins["down"] <= step:
+                turn = turn_of[step - begins["down"]]
+                for pack in packs_of[4]:
+                    arrive(pack, *turn, out)
+                    if turn != (0, 0):
+                        out.append(("handed", pack, *turn))
+            gaps.append(out)
+        return gaps, sends
+
+    programs = [actions(plan, at >= 2, at % 2 == 1) for at, plan in enumerate(PLANS)]
+
+    def act(todo):
+        for kind, *rest in todo:
+            if kind == "load":
+                for one in loads[rest[0]]:
+                    one.wait()
+                continue
+            at = spots[rest[2]][rest[1]]
+            if kind == "arrive":
+                copy(rest[0], at, CORE).wait_recv()
+            elif kind == "handed":
+                copy(rest[0], at, CORE, 1 - core).wait_recv()
+            elif kind == "send":
+                copy(rest[0], at, rest[3]).start()
+            else:
+                copy(rest[0], at, rest[3]).wait_send()
+
+    def ahead_of(step, index=None):
+        for mine, (gaps, _) in zip(roles, programs):
+            if gaps[step]:
+                asked = mine if index is None else jnp.logical_and(mine, index == step - begins[steps[step]])
+                pl.when(asked)(functools.partial(act, gaps[step]))
+
+    def loop(name, length, body):
+        def whole(index, _):
+            for step in range(begins[name], begins[name] + length):
+                ahead_of(step, index)
+            body(index)
+
+        lax.fori_loop(0, length, whole, None)
+
+    drained = [set() for _ in programs]
+
+    def drain(weights, before):
+        for mine, (_, sends), gone in zip(roles, programs, drained):
+            now = [one for one in sends if PACKS[one[0]][0] in weights and one[-1] < before and one not in gone]
+            gone.update(now)
+            pl.when(mine)(functools.partial(act, [("sent", *one) for one in now]))
+
+    for group in loads:
+        for one in group:
+            one.start()
     barrier = pltpu.get_barrier_semaphore()
     for target in [targets[LINE], targets[SIDE], targets[CORE], across]:
         pl.semaphore_signal(barrier, inc=1, device_id=target, device_id_type=MESH)
@@ -264,38 +342,17 @@
 
     pl.semaphore_wait(barrier, 4 + z * (3 - z) // 2)
 
-    loads["a0"].wait()
-    loads["a1"].wait()
-    send_own(0)
-    loads["b"].wait()
-    send_own(1)
-    run(events(0)[:5])
-    for name in ("c0", "c1"):
-        loads[name].wait()
-    send_own(2)
-    run(events(0)[5:])
-    all_handed(0)
-    loads["tok"].wait()
-    loads["shift"].wait()
-
-    block = rate_ref.shape[1]
-
-    def recur_step(i, plan):
+    def recur_step(i):
         cols = pl.ds(pl.multiple_of(i * block, block), block)
         value_in = jnp.dot(tok[...], buf_a[0, :, cols], preferred_element_type=jnp.float32)
         gate_in = jnp.dot(tok[...], buf_a[1, :, cols], preferred_element_type=jnp.float32)
+        param = -param_ref[:, cols]
+        plus = jnp.maximum(param, 0.0) + jnp.log1p(jnp.exp(-jnp.abs(param)))
         branch[:, cols] = recur_core(
-            value_in, gate_in, taps_ref[:, cols], rate_ref[i], inlet_ref[i], plus_ref[:, cols], shift[:, cols]
+            value_in, gate_in, taps_ref[:, cols], rate_blocks[i], inlet_blocks[i], plus, shift[:, cols]
         )
-        at_step(i, plan)
-
-    ev = events(1)
-    plan = [ev[:2], ev[2:4], ev[4:5], ev[5:]]
-    lax.fori_loop(0, rate_ref.shape[0], lambda i, _: recur_step(i, plan), None)
-    for name in ("c2", "c3"):
-        loads[name].wait()
-    send_own(3)
-    all_handed(1)
+
+    loop("recur", blocks, recur_step)
 
     def terms_copy(phase, at):
         return pltpu.make_async_remote_copy(
@@ -312,27 +369,22 @@
         for row in range(2):
             terms[row, at] = product[row * share : (row + 1) * share]
 
-    parts = buf_b.shape[0]
-
-    def mix_step(s, _):
+    def mix_step(s):
         keep(jnp.dot(branch[...], buf_b[s], preferred_element_type=jnp.float32), s)
         pl.when(s > 0)(lambda: terms_copy(0, s - 1).start())
 
-    lax.fori_loop(0, parts, mix_step, None)
-    ev = events(2)
-    run(ev[:1])
+    loop("mix", parts, mix_step)
+    drain([0], begins["recur"] + 1)
     terms_copy(0, parts - 1).start()
-    run(ev[1:2])
+    ahead_of(begins["terms"])
     for s in range(parts):
         terms_copy(0, s).wait_recv()
 
-    rows = 64
-
     def norm_rows(i, phase, residual, gain_ref):
-        piece_rows = pl.ds(pl.multiple_of(i * rows, rows), rows)
+        here = pl.ds(pl.multiple_of(i * rows, rows), rows)
         value = jnp.concatenate(
             [
-                terms[tp, s, piece_rows, :].astype(jnp.float32) + came[phase, s, piece_rows, :].astype(jnp.float32)
+                terms[tp, s, here, :].astype(jnp.float32) + came[phase, s, here, :].astype(jnp.float32)
                 for s in range(parts)
             ],
             axis=1,
@@ -352,46 +404,30 @@
             device_id_type=MESH,
         )
 
-    def first_norm(i, _):
+    def first_norm(i):
         normed[own_rows(i), :] = norm_rows(i, 0, tok[own_rows(i), :], first_gain_ref)
         pl.when(i > 0)(lambda: norm_copy(i - 1).start())
 
-    tiles = share // rows
-    lax.fori_loop(0, tiles, first_norm, None)
-    run(ev[2:3])
-    norm_copy(tiles - 1).start()
-    run(ev[3:5])
-    loads["d"].wait()
-    send_own(4)
-    run(ev[5:])
-    for i in range(tiles):
+    loop("norm", row_tiles, first_norm)
+    drain([1], begins["terms"])
+    for s in range(parts):
+        terms_copy(0, s).wait_send()
+    norm_copy(row_tiles - 1).start()
+    ahead_of(begins["rows"])
+    for i in range(row_tiles):
         norm_copy(i).wait_recv()
-    all_handed(2)
-
-    def hidden_step(j, half, plan):
+
+    def hidden_step(j, half):
         cols = pl.ds(pl.multiple_of(j * tile, tile), tile)
         gate = jnp.dot(normed[...], buf_c[half, 0, :, cols], preferred_element_type=jnp.float32)
         upward = jnp.dot(normed[...], buf_c[half, 1, :, cols], preferred_element_type=jnp.float32)
         to = pl.ds(pl.multiple_of(half * ff_half + j * tile, tile), tile)
         hidden[:, to] = (gate * sigmoid(gate) * upward).astype(jnp.bfloat16)
-        at_step(j, plan)
-
-    steps = ff_half // tile
-    ev = events(3)
-    plan = [ev[:2], ev[2:3], ev[3:4], ev[4:5], []]
-    lax.fori_loop(0, steps, lambda j, _: hidden_step(j, 0, plan), None)
-    send_own(5)
-    run(ev[5:])
-    all_handed(3)
-    ev = events(4)
-    plan = [ev[:2], ev[2:3], ev[3:5], ev[5:6], []]
-    lax.fori_loop(0, steps, lambda j, _: hidden_step(j, 1, plan), None)
-    run(ev[6:])
-
-    for s in range(parts):
-        terms_copy(0, s).wait_send()
-
-    ev = events(5)
+
+    loop("hidden0", tiles, lambda j: hidden_step(j, 0))
+    loop("hidden1", tiles, lambda j: hidden_step(j, 1))
+
+    order = [spots[side][k] for k, side in turn_of]
 
     def pick(j):
         at = order[0]
@@ -399,20 +435,17 @@
             at = jnp.where(j == turn, order[turn], at)
         return at
 
-    def down_step(j, _):
-        at_step(j, [[]] + [[e] for e in ev])
+    def down_step(j):
         at = pick(j)
-        @pl.when(j > 0)
-        def _():
-            handed(4, at)
-            handed(5, at)
         keep(jnp.dot(hidden[...], buf_d[at], preferred_element_type=jnp.float32), at)
         pl.when(j > 0)(lambda: terms_copy(1, pick(j - 1)).start())
 
-    lax.fori_loop(0, parts, down_step, None)
-    for pack, at, way, condition in sent:
-        under(condition, lambda: copy(pack, at, way).wait_send())
+    loop("down", parts, down_step)
+    drain(range(3), len(steps))
     terms_copy(1, order[-1]).start()
+    drain(range(5), len(steps))
+    for i in range(row_tiles):
+        norm_copy(i).wait_send()
     for s in order:
         terms_copy(1, s).wait_recv()
 
@@ -420,9 +453,7 @@
         here = pl.ds(pl.multiple_of(i * rows, rows), rows)
         out_ref[here, :] = norm_rows(i, 1, normed[own_rows(i), :], second_gain_ref)
 
-    lax.fori_loop(0, tiles, second_norm, None)
-    for i in range(tiles):
-        norm_copy(i).wait_send()
+    lax.fori_loop(0, row_tiles, second_norm, None)
     for s in range(parts):
         terms_copy(1, s).wait_send()
 
@@ -452,9 +483,11 @@
     hbm = pl.BlockSpec(memory_space=pl.ANY)
     vmem = pl.BlockSpec(memory_space=pltpu.VMEM)
     half = jnp.bfloat16
+    packs = len(PACKS)
+    row_tiles = share // min(64, share)
     return pl.pallas_call(
         layer_kernel,
-        in_specs=[hbm, hbm, hbm, vmem, vmem, vmem, vmem, hbm, hbm, vmem, hbm, hbm, hbm, vmem],
+        in_specs=[hbm, hbm, hbm, vmem, hbm, hbm, vmem, hbm, hbm, vmem, hbm, hbm, hbm, vmem],
         out_specs=vmem,
         out_shape=jax.ShapeDtypeStruct((share, model), half),
         scratch_shapes=[
@@ -463,19 +496,21 @@
             pltpu.VMEM((2, 2, depth * parts, units // 2), half),
             pltpu.VMEM((parts, units, columns), half),
             pltpu.VMEM((length, model), half),
+            pltpu.VMEM(recurrence_gate_blockwise.shape, half),
+            pltpu.VMEM(input_gate_blockwise.shape, half),
             pltpu.VMEM((length, channels), jnp.float32),
             pltpu.VMEM((length, channels), half),
             pltpu.VMEM((2, parts, share, columns), half),
             pltpu.VMEM((2, parts, share, columns), half),
             pltpu.VMEM((length, model), half),
             pltpu.VMEM((length, units), half),
-            pltpu.SemaphoreType.DMA((10,)),
-            pltpu.SemaphoreType.DMA((6, parts, 4)),
-            pltpu.SemaphoreType.DMA((6, 2, parts)),
+            pltpu.SemaphoreType.DMA((12,)),
+            pltpu.SemaphoreType.DMA((packs, parts, 4)),
+            pltpu.SemaphoreType.DMA((packs, 2, parts)),
             pltpu.SemaphoreType.DMA((2, parts)),
             pltpu.SemaphoreType.DMA((2, parts)),
-            pltpu.SemaphoreType.DMA((share // 64,)),
-            pltpu.SemaphoreType.DMA((share // 64,)),
+            pltpu.SemaphoreType.DMA((row_tiles,)),
+            pltpu.SemaphoreType.DMA((row_tiles,)),
         ],
         cost_estimate=pl.CostEstimate(
             flops=2 * length * model * (2 * channels + 2 * units) + 2 * length * model * (channels + units),
@@ -492,7 +527,7 @@
         convolution_kernel,
         recurrence_gate_blockwise,
         input_gate_blockwise,
-        jax.nn.softplus(-channel_decay_param)[None, :],
+        channel_decay_param[None, :],
         token_decay_shift,
         recurrence_output_weight,
         first_norm_gain[None, :],

time: 264 us -> 246 us (0.932)
  Pallas kernels: 260 us -> 244 us
    pallas_call x1, Pallas kernels: 260 us -> 244 us  [whole_layer(): pl.pallas_call(layer_kernel, in_specs=[hbm, hbm, hbm, vmem, hbm, hbm, vme...]
where the time goes in v1:
time: 246 us
  Pallas kernels  244 us (99%)
    pallas_call x1, Pallas kernels, whole_layer(): pl.pallas_call(layer_kernel, in_specs=[hbm, hbm, hbm, vmem, hbm, hbm, vme...  244 us

profile of v1, /device:TPU:0, one launch (start us, length us, event | category | flops | bytes accessed | tf_op | source)
XLA Modules:
  0.0 246.2 jit_solution(12594779512381528482)
XLA Ops:
  0.0 243.9 %shard_map.136 = bf16[256,2048]{1,0:T(8,128)(2,1)} custom-call(bf16[512,2048]{1,0:T(8,128)(2,1)} %tok_hbm.1, bf16[256,1024]{1,0:T(8,128)(2,1)} %in_hbm.1, bf16[256,1024]{1,0:T(8,128)(2,1)} %gate_hbm.1, bf16[4,1024]{1,0:T(4,128)(2,1)} %taps_ref.1, bf16[4,256,256]{2,1,0:T(8,128)(2,1)} %rate_hbm.1, bf16[4,256,256]{2,1,0:T(8,128)(2,1)} %inlet_hbm.1, ...), custom_call_target="tpu_custom_call" | custom-call | flops 22548578304 | bytes 44040192 | tf_op jit(solution)/shard_map/pallas_call | solution.py:488
  243.9 2.3 copy.16

commit v2 on v1

--- a/solution.py
+++ b/solution.py
@@ -78,38 +78,44 @@
 
 
 LINE, OTHER, SIDE, CORE = 0, 1, 2, 3
+INPUTS = 7
 OWN, OWN_SIDE, FROM_SIDE, FROM_LINE, ON_SIDE, FROM_FAR_SIDE = range(6)
-PACKS = ((0, 0, 1), (1, 0, 1), (2, 0, 1), (3, 0, 1), (4, 0, 2), (4, 1, 2))
+A_PARTS = 1
+PACKS = ((0, 0, 1), (2, 0, 1), (3, 0, 1), (4, 0, 1), (5, 0, 2), (5, 1, 2), (6, 0, 1))
+ALONG = ((1, 1), (1, 1), (0, 0), (1, 1), (0, 0), (1, 1), (1, 1))
 PLANS = (
     (
-        (100, 110, 0, 10, 401, 130, 402, 403),
-        (503, 412, 303, 200, 312, 210, 20, 501, 413, 30, 150, 502, 431, 411, 313, 302, 421, 120, 512),
-        (50, 311, 511, 513, 301), (432,), (), (), (331, 322), (), (321,), (422,), (220, 40, 451), (230, 423), (),
-        (521,), (433, 341), (523,), (351, 522, 333, 140), (441,), (323, 533, 532), (), (), (332,), (), (531, 442),
-        (), (), (250, 452), (342,), (352,), (240, 443, 551, 541), (343,), (543,), (353, 453, 552), (542,), (553,),
-        (),
+        (110, 331, 130, 10, 160, 421, 0, 402, 100, 200, 20, 403, 502, 531, 301, 522, 333, 210, 60, 311),
+        (501, 503, 302, 50, 431), (30, 230, 451, 412, 303), (413, 401), (513, 312, 512, 511, 120), (40,), (140,), (),
+        (), (341,), (), (332,), (441, 260, 313), (351,), (), (150,), (), (), (), (), (523, 461), (342,), (442, 453),
+        (), (), (452, 240), (553, 343, 541), (), (), (443, 321), (542,), (), (551,), (361, 352, 411), (), (), (533,),
+        (353,), (), (), (), (250, 323, 462, 552, 543), (220, 362), (), (363,), (), (), (562, 423, 532, 322), (433,),
+        (521, 463, 561), (), (563,), (), (), (422, 432),
     ),
     (
 
-        (130, 100, 0, 10, 301, 20, 200, 403, 110, 401, 503, 402, 302, 421, 120, 412, 303, 312, 501, 150, 502, 210, 411),
-        (413,), (313, 50), (311, 512, 40, 513, 511, 432), (), (), (), (), (322, 30), (140,), (331,), (422,),
-        (451, 230), (332,), (), (), (), (220, 321, 323, 522, 423, 521), (531,), (351, 441), (532, 431),
-        (523, 333, 433, 533), (442, 250), (), (240,), (), (342, 452), (), (), (352,), (), (551, 552),
-        (341, 443, 343, 541), (353, 542, 453, 543), (), (553,),
+        (522, 110, 100, 0, 130, 160, 60, 331, 333, 10, 50, 20, 210, 200, 531, 301, 402, 230, 30, 421, 40, 502, 501, 302, 401, 403, 451, 503, 413, 303, 311, 412, 120, 512, 313, 312, 513, 511, 361),
+        (260,), (), (), (140, 441), (523,), (), (442,), (), (341, 150), (), (), (), (453,), (), (), (452,),
+        (431, 332, 461), (), (323, 443), (), (), (411, 553, 240, 343, 352, 321, 250, 322, 541, 342), (), (), (), (),
+        (), (), (542,), (), (463,), (), (462, 351, 423, 533, 353), (), (521, 432, 551), (), (552,), (543,), (), (),
+        (362, 363), (), (), (), (532,), (), (), (433,), (), (), (), (422, 561, 563), (562,), (220,),
     ),
     (
-        (0, 100, 110, 401, 301, 311, 10, 302, 403, 130, 303, 402), (313, 312, 501, 210, 503, 30, 150),
-        (200, 412, 20, 411, 502, 50), (120, 413), (512, 513, 511), (432,), (332,), (), (422,), (322,), (331,),
-        (140, 321), (451,), (230, 323, 431, 423), (), (), (351,), (341, 421),
-        (523, 522, 220, 333, 441, 531, 40, 250, 532, 521), (433,), (), (), (533,), (342,), (352, 452), (),
-        (343, 240, 442), (), (443, 551), (), (543, 552, 541), (542, 353, 453), (553,), (), (), (),
+        (140, 0, 150, 10, 311, 302, 301, 110, 100, 403, 303, 210, 200, 451, 20, 413, 402), (130, 501, 503),
+        (502, 511, 240, 312, 512, 313), (120, 40), (), (), (351,), (), (50,), (422, 421, 331, 513), (442,),
+        (342, 321, 401), (30,), (353,), (), (230, 341, 160), (60,), (433, 521, 531), (332,), (),
+        (423, 333, 250, 361, 352), (323, 523), (441, 533, 343, 453, 443, 522, 220, 532), (), (322, 362), (561,),
+        (542,), (541, 260), (), (), (), (), (), (363, 461, 463, 552), (), (), (), (), (), (431,), (562, 543), (), (),
+        (553, 551), (), (), (), (), (), (411,), (), (), (), (412,), (432, 452, 563, 462),
     ),
     (
-        (100, 401, 0, 10, 110, 302, 311, 402, 312, 301, 303, 403, 501, 413, 200, 20, 30, 503, 502, 150), (), (411,),
-        (), (210, 313, 332, 50, 412, 321, 130, 513, 511), (), (120,), (), (512,), (422, 322, 40, 331), (323,),
-        (230, 451, 140, 423), (), (), (), (220,), (521,), (421, 432, 433, 523), (522,), (441, 531), (), (333,),
-        (351, 342, 532), (), (250, 352), (533,), (), (341, 431, 443, 442), (551, 240), (), (343, 552), (), (),
-        (543, 353, 453, 542), (), (452, 541, 553),
+
+        (100, 130, 0, 302, 110, 150, 200, 301, 10, 120, 403, 502, 303, 311, 401, 413, 313, 501, 160, 60, 503, 511, 140, 441, 402, 210, 312, 321, 512, 451, 20),
+        (513, 40, 362), (), (50,), (), (422, 421, 351), (), (), (), (342, 442, 30), (353, 240), (), (220,),
+        (521, 352, 331), (), (332,), (531, 341, 423), (461,), (), (230, 522, 322, 323, 361, 433, 443, 523, 333),
+        (343, 533, 532, 250, 542, 453), (363,), (), (561, 553, 543, 541), (551, 552), (), (), (), (260,), (), (),
+        (463,), (431,), (), (), (), (563, 562), (), (), (), (), (), (), (411,), (), (), (), (), (412,), (), (), (),
+        (), (), (452, 462, 432),
     ),
 )
 
@@ -132,6 +138,8 @@
     out_ref,
     buf_a,
     buf_b,
+    buf_e,
+    buf_f,
     buf_c,
     buf_d,
     tok,
@@ -150,6 +158,11 @@
     terms_recv,
     norm_send,
     norm_recv,
+    far_send,
+    far_recv,
+    back_send,
+    back_recv,
+    free_sem,
 ):
     core, fs, tp = lax.axis_index("rep"), lax.axis_index("fs"), lax.axis_index("tp")
     z, y = fs // 2, fs % 2
@@ -157,6 +170,7 @@
     middle = z * (3 - z) == 2
     role = core + z * (3 - z)
     roles = [role == at for at in range(4)]
+    outer = jnp.logical_not(middle)
     spots = [[k * 2 + y for k in zs], [k * 2 + 1 - y for k in zs]]
     me = spots[0][0]
     targets = {
@@ -168,13 +182,14 @@
     across = (core, me, 1 - tp)
     width = in_hbm.shape[0]
     parts = buf_b.shape[0]
-    ff_half = buf_c.shape[3]
-    mix_depth, down_depth = buf_b.shape[1], buf_d.shape[1]
+    first_units, other_units = buf_e.shape[2], buf_c.shape[2]
+    a_columns = buf_a.shape[3]
+    mix_depth = buf_b.shape[1]
     share = out_ref.shape[0]
     block = rate_blocks.shape[1]
     blocks = rate_blocks.shape[0]
-    tile = min(256, ff_half)
-    tiles = ff_half // tile
+    tile = min(256, first_units)
+    first_tiles, other_tiles = first_units // tile, other_units // tile
     rows = min(64, share)
     row_tiles = share // rows
     own_row = pl.multiple_of(tp * share, share)
@@ -184,13 +199,19 @@
 
     def piece(pack, at, half):
         weight, part, count = PACKS[pack]
-        if weight == 0:
-            return buf_a.at[half, run_of(at * width, part, width // count), :]
-        if weight == 1:
-            return buf_b.at[at, run_of(half * (mix_depth // 2), part, mix_depth // 2 // count), :]
-        if weight < 4:
-            return buf_c.at[weight - 2, half, run_of(at * width, part, width // count), :]
-        return buf_d.at[at, run_of(half * (down_depth // 2), part, down_depth // 2 // count), :]
+        by_row = run_of(at * width, part, width // count)
+        by_depth = lambda depth: run_of(half * (depth // 2), part, depth // 2 // count)
+        if weight < 2:
+            return buf_a.at[weight, half, by_row, :]
+        if weight == 2:
+            return buf_b.at[at, by_depth(mix_depth), :]
+        if weight == 3:
+            return buf_e.at[half, by_row, :]
+        if weight == 4:
+            return buf_f.at[at, by_depth(first_units), :]
+        if weight == 5:
+            return buf_c.at[half, by_row, :]
+        return buf_d.at[at, by_depth(other_units), :]
 
     def copy(pack, at, way, half=core):
         return pltpu.make_async_remote_copy(
@@ -202,14 +223,22 @@
             device_id_type=MESH,
         )
 
-    c_cols = lambda half: pl.ds(half * ff_half, ff_half)
     own_rows_of = lambda ref, *at: ref.at[(*at, pl.ds(pl.multiple_of(me * width, width), width), slice(None))]
+    a_part = lambda part: [
+        (ref.at[:, pl.ds(part * a_columns, a_columns)], own_rows_of(buf_a, part, half))
+        for half, ref in enumerate((in_hbm, gate_hbm))
+    ]
+    units_of = lambda start, count, buf: [
+        (ref.at[:, pl.ds(start, count)], own_rows_of(buf, half)) for half, ref in enumerate((ffgate_hbm, ffup_hbm))
+    ]
     loads = [
-        [(in_hbm, own_rows_of(buf_a, 0)), (gate_hbm, own_rows_of(buf_a, 1))],
+        a_part(0),
+        a_part(1) if A_PARTS == 2 else [],
         [(out_hbm, buf_b.at[me])],
-        [(ffgate_hbm.at[:, c_cols(0)], own_rows_of(buf_c, 0, 0)), (ffup_hbm.at[:, c_cols(0)], own_rows_of(buf_c, 0, 1))],
-        [(ffgate_hbm.at[:, c_cols(1)], own_rows_of(buf_c, 1, 0)), (ffup_hbm.at[:, c_cols(1)], own_rows_of(buf_c, 1, 1))],
-        [(down_hbm, buf_d.at[me])],
+        units_of(0, first_units, buf_e),
+        [(down_hbm.at[pl.ds(0, first_units), :], buf_f.at[me])],
+        units_of(first_units, other_units, buf_c),
+        [(down_hbm.at[pl.ds(first_units, other_units), :], buf_d.at[me])],
         [(tok_hbm, tok), (shift_hbm, shift), (rate_hbm, rate_blocks), (inlet_hbm, inlet_blocks)],
     ]
     count = 0
@@ -218,12 +247,15 @@
             group[at] = pltpu.make_async_copy(source, target, load_sem.at[count])
             count += 1
 
-    steps = ["recur"] * blocks + ["mix"] * parts + ["terms"] + ["norm"] * row_tiles + ["rows"]
-    steps += ["hidden0"] * tiles + ["hidden1"] * tiles + ["down"] * parts
+    steps = ["recur"] * blocks + ["mix"] * parts + ["terms"] + ["norm"] * row_tiles + ["rows"] * row_tiles
+    steps += ["first"] * first_tiles + ["far"] * parts + ["back"] * parts
+    steps += ["hidden"] * other_tiles + ["down"] * parts
     begins = {name: steps.index(name) for name in dict.fromkeys(steps)}
     turn_of = [(0, 0), (0, 1), (1, 0), (2, 0), (1, 1), (3, 0), (2, 1), (3, 1)]
-    needs = {begins["recur"]: 0, begins["mix"]: 1, begins["hidden0"]: 2, begins["hidden1"]: 3}
-    packs_of = [[p for p, (w, _, _) in enumerate(PACKS) if w == weight] for weight in range(5)]
+    needs = {begins["recur"]: 0, begins["mix"]: 2, begins["first"]: 3, begins["far"]: 4, begins["hidden"]: 5}
+    if A_PARTS == 2:
+        needs[begins["recur"] + blocks // 2] = 1
+    packs_of = [[p for p, (w, _, _) in enumerate(PACKS) if w == weight] for weight in range(INPUTS)]
 
     def actions(plan, in_middle, second):
         loaded, waited, sends, gaps = set(), set(), [], []
@@ -249,25 +281,32 @@
             out = []
             for code in codes:
                 kind, pack, k = code // 100, code // 10 % 10, code % 10
+                first = PACKS[pack][0] in (3, 4)
+                along = ALONG[pack][second]
                 if kind == OWN:
-                    send(pack, 0, 0, LINE, out)
+                    if not (first and in_middle):
+                        send(pack, 0, 0, LINE, out)
                     if in_middle:
                         send(pack, 0, 0, OTHER, out)
                 elif kind == OWN_SIDE:
-                    send(pack, 0, 0, SIDE, out)
+                    if not first or in_middle or along:
+                        send(pack, 0, 0, SIDE, out)
                 elif kind == FROM_SIDE:
-                    arrive(pack, 0, 1, out)
-                    if second:
-                        send(pack, 0, 1, LINE, out)
+                    if along:
+                        if not (first and in_middle):
+                            send(pack, 0, 1, LINE, out)
                         if in_middle:
                             send(pack, 0, 1, OTHER, out)
-                    send(pack, 0, 1, CORE, out)
+                    if not first or in_middle:
+                        send(pack, 0, 1, CORE, out)
+                elif first and not in_middle:
+                    pass
                 elif kind == FROM_LINE:
-                    if in_middle:
+                    if in_middle and (k == 1 or not first):
                         send(pack, k, 0, OTHER if k == 1 else LINE, out)
                     send(pack, k, 0, CORE, out)
                 elif kind == ON_SIDE:
-                    if k == 3 or not second or (k == 2 and not in_middle):
+                    if k == 3 or not along or (k == 2 and not in_middle):
                         send(pack, k, 0, SIDE, out)
                 else:
                     send(pack, k, 1, CORE, out)
@@ -275,21 +314,21 @@
                 weight = needs[step]
                 load(weight, out)
                 if step == 0:
-                    load(5, out)
-                for pack in packs_of[weight]:
+                    load(INPUTS, out)
+                for pack in packs_of[weight] if in_middle or weight not in (3, 4) else []:
                     for turn in turn_of[1:]:
                         arrive(pack, *turn, out)
                         out.append(("handed", pack, *turn))
             if begins["down"] <= step:
                 turn = turn_of[step - begins["down"]]
-                for pack in packs_of[4]:
+                for pack in packs_of[6]:
                     arrive(pack, *turn, out)
                     if turn != (0, 0):
                         out.append(("handed", pack, *turn))
             gaps.append(out)
         return gaps, sends
 
-    programs = [actions(plan, at >= 2, at % 2 == 1) for at, plan in enumerate(PLANS)]
+    programs = [actions(plan, at >= 2, at % 2) for at, plan in enumerate(PLANS)]
 
     def act(todo):
         for kind, *rest in todo:
@@ -344,8 +383,9 @@
 
     def recur_step(i):
         cols = pl.ds(pl.multiple_of(i * block, block), block)
-        value_in = jnp.dot(tok[...], buf_a[0, :, cols], preferred_element_type=jnp.float32)
-        gate_in = jnp.dot(tok[...], buf_a[1, :, cols], preferred_element_type=jnp.float32)
+        part, place = (i * block) // a_columns, pl.ds(pl.multiple_of(i * block % a_columns, block), block)
+        value_in = jnp.dot(tok[...], buf_a[part, 0, :, place], preferred_element_type=jnp.float32)
+        gate_in = jnp.dot(tok[...], buf_a[part, 1, :, place], preferred_element_type=jnp.float32)
         param = -param_ref[:, cols]
         plus = jnp.maximum(param, 0.0) + jnp.log1p(jnp.exp(-jnp.abs(param)))
         branch[:, cols] = recur_core(
@@ -357,7 +397,7 @@
     def terms_copy(phase, at):
         return pltpu.make_async_remote_copy(
             src_ref=terms.at[1 - tp, at],
-            dst_ref=came.at[phase, at],
+            dst_ref=came.at[phase % 2, at],
             send_sem=terms_send.at[phase, at],
             recv_sem=terms_recv.at[phase, at],
             device_id=across,
@@ -374,7 +414,7 @@
         pl.when(s > 0)(lambda: terms_copy(0, s - 1).start())
 
     loop("mix", parts, mix_step)
-    drain([0], begins["recur"] + 1)
+    drain([0, 1], begins["recur"] + 1)
     terms_copy(0, parts - 1).start()
     ahead_of(begins["terms"])
     for s in range(parts):
@@ -382,13 +422,12 @@
 
     def norm_rows(i, phase, residual, gain_ref):
         here = pl.ds(pl.multiple_of(i * rows, rows), rows)
-        value = jnp.concatenate(
-            [
-                terms[tp, s, here, :].astype(jnp.float32) + came[phase, s, here, :].astype(jnp.float32)
-                for s in range(parts)
-            ],
-            axis=1,
-        )
+
+        def total(s):
+            value = terms[tp, s, here, :].astype(jnp.float32) + came[phase, s, here, :].astype(jnp.float32)
+            return value if phase == 0 else value + jnp.where(outer, came[0, s, here, :].astype(jnp.float32), 0.0)
+
+        value = jnp.concatenate([total(s) for s in range(parts)], axis=1)
         return layer_norm(residual_scale * residual.astype(jnp.float32) + value, gain_ref[...]).astype(jnp.bfloat16)
 
     def own_rows(i):
@@ -404,28 +443,100 @@
             device_id_type=MESH,
         )
 
+    def far_copy(half, i):
+        here = pl.ds(pl.multiple_of(half * share + i * rows, rows), rows)
+        return pltpu.make_async_remote_copy(
+            src_ref=normed.at[here, :],
+            dst_ref=tok.at[here, :],
+            send_sem=far_send.at[half, i],
+            recv_sem=far_recv.at[half, i],
+            device_id=targets[LINE],
+            device_id_type=MESH,
+        )
+
+    def pass_on(i):
+        norm_copy(i).start()
+        pl.when(outer)(lambda: far_copy(tp, i).start())
+
     def first_norm(i):
         normed[own_rows(i), :] = norm_rows(i, 0, tok[own_rows(i), :], first_gain_ref)
-        pl.when(i > 0)(lambda: norm_copy(i - 1).start())
+        pl.when(jnp.logical_and(outer, i == 1))(lambda: pl.semaphore_wait(free_sem, 1))
+        pl.when(i > 0)(lambda: pass_on(i - 1))
 
     loop("norm", row_tiles, first_norm)
-    drain([1], begins["terms"])
+    drain([2], begins["terms"])
     for s in range(parts):
         terms_copy(0, s).wait_send()
-    norm_copy(row_tiles - 1).start()
-    ahead_of(begins["rows"])
+
+    @pl.when(middle)
+    def _():
+        pl.semaphore_signal(free_sem, inc=1, device_id=targets[LINE], device_id_type=MESH)
+
+    pass_on(row_tiles - 1)
     for i in range(row_tiles):
+        ahead_of(begins["rows"] + i)
         norm_copy(i).wait_recv()
-
-    def hidden_step(j, half):
+        pl.when(outer)(lambda i=i: far_copy(1 - tp, i).start())
+
+    def units_at(left, buf, j):
         cols = pl.ds(pl.multiple_of(j * tile, tile), tile)
-        gate = jnp.dot(normed[...], buf_c[half, 0, :, cols], preferred_element_type=jnp.float32)
-        upward = jnp.dot(normed[...], buf_c[half, 1, :, cols], preferred_element_type=jnp.float32)
-        to = pl.ds(pl.multiple_of(half * ff_half + j * tile, tile), tile)
-        hidden[:, to] = (gate * sigmoid(gate) * upward).astype(jnp.bfloat16)
-
-    loop("hidden0", tiles, lambda j: hidden_step(j, 0))
-    loop("hidden1", tiles, lambda j: hidden_step(j, 1))
+        gate = jnp.dot(left[...], buf[0, :, cols], preferred_element_type=jnp.float32)
+        upward = jnp.dot(left[...], buf[1, :, cols], preferred_element_type=jnp.float32)
+        return (gate * sigmoid(gate) * upward).astype(jnp.bfloat16)
+
+    def in_middle(body):
+        def asked(i):
+            pl.when(middle)(lambda: body(i))
+
+        return asked
+
+    def first_step(j):
+        @pl.when(j == 0)
+        def _():
+            for half in range(2):
+                for i in range(row_tiles):
+                    far_copy(half, i).wait_recv()
+
+        to = pl.ds(pl.multiple_of(j * tile, tile), tile)
+        hidden[:, to] = units_at(normed, buf_e, j)
+        branch[:, to] = units_at(tok, buf_e, j)
+
+    def far_step(s):
+        left = branch[:, :first_units]
+        keep(jnp.dot(left, buf_f[s], preferred_element_type=jnp.float32), s)
+        pl.when(s > 0)(lambda: terms_copy(2, s - 1).start())
+
+    def back_copy(s):
+        return pltpu.make_async_remote_copy(
+            src_ref=came.at[0, s],
+            dst_ref=came.at[0, s],
+            send_sem=back_send.at[s],
+            recv_sem=back_recv.at[s],
+            device_id=targets[LINE],
+            device_id_type=MESH,
+        )
+
+    def back_step(s):
+        pl.when(s == 0)(lambda: terms_copy(2, parts - 1).start())
+        terms_copy(2, s).wait_recv()
+        came[0, s] = (terms[tp, s].astype(jnp.float32) + came[0, s].astype(jnp.float32)).astype(jnp.bfloat16)
+        pl.when(s > 0)(lambda: back_copy(s - 1).start())
+
+    loop("first", first_tiles, in_middle(first_step))
+    loop("far", parts, in_middle(far_step))
+    loop("back", parts, in_middle(back_step))
+
+    @pl.when(middle)
+    def _():
+        for s in range(parts):
+            terms_copy(2, s).wait_send()
+        back_copy(parts - 1).start()
+
+    def hidden_step(j):
+        to = pl.ds(pl.multiple_of(first_units + j * tile, tile), tile)
+        hidden[:, to] = units_at(normed, buf_c, j)
+
+    loop("hidden", other_tiles, hidden_step)
 
     order = [spots[side][k] for k, side in turn_of]
 
@@ -437,15 +548,32 @@
 
     def down_step(j):
         at = pick(j)
-        keep(jnp.dot(hidden[...], buf_d[at], preferred_element_type=jnp.float32), at)
+        product = lambda: jnp.dot(hidden[:, first_units:], buf_d[at], preferred_element_type=jnp.float32)
+        more = lambda: jnp.dot(hidden[:, :first_units], buf_f[at], preferred_element_type=jnp.float32)
+        pl.when(outer)(lambda: keep(product(), at))
+        pl.when(middle)(lambda: keep(product() + more(), at))
         pl.when(j > 0)(lambda: terms_copy(1, pick(j - 1)).start())
 
     loop("down", parts, down_step)
-    drain(range(3), len(steps))
+    drain(range(5), len(steps))
     terms_copy(1, order[-1]).start()
-    drain(range(5), len(steps))
+    drain(range(INPUTS), len(steps))
     for i in range(row_tiles):
         norm_copy(i).wait_send()
+
+    @pl.when(outer)
+    def _():
+        for half in range(2):
+            for i in range(row_tiles):
+                far_copy(half, i).wait_send()
+        for s in range(parts):
+            back_copy(s).wait_recv()
+
+    @pl.when(middle)
+    def _():
+        for s in range(parts):
+            back_copy(s).wait_send()
+
     for s in order:
         terms_copy(1, s).wait_recv()
 
@@ -479,6 +607,7 @@
     share = length // lax.axis_size("tp")
     depth, channels = recurrence_branch_weight.shape
     units = feedforward_gate_weight.shape[1]
+    first_units = units * 2 // 5 // 256 * 256
     columns = recurrence_output_weight.shape[1]
     hbm = pl.BlockSpec(memory_space=pl.ANY)
     vmem = pl.BlockSpec(memory_space=pltpu.VMEM)
@@ -491,10 +620,12 @@
         out_specs=vmem,
         out_shape=jax.ShapeDtypeStruct((share, model), half),
         scratch_shapes=[
-            pltpu.VMEM((2, depth * parts, channels), half),
+            pltpu.VMEM((A_PARTS, 2, depth * parts, channels // A_PARTS), half),
             pltpu.VMEM((parts, channels, columns), half),
-            pltpu.VMEM((2, 2, depth * parts, units // 2), half),
-            pltpu.VMEM((parts, units, columns), half),
+            pltpu.VMEM((2, depth * parts, first_units), half),
+            pltpu.VMEM((parts, first_units, columns), half),
+            pltpu.VMEM((2, depth * parts, units - first_units), half),
+            pltpu.VMEM((parts, units - first_units, columns), half),
             pltpu.VMEM((length, model), half),
             pltpu.VMEM(recurrence_gate_blockwise.shape, half),
             pltpu.VMEM(input_gate_blockwise.shape, half),
@@ -504,13 +635,18 @@
             pltpu.VMEM((2, parts, share, columns), half),
             pltpu.VMEM((length, model), half),
             pltpu.VMEM((length, units), half),
-            pltpu.SemaphoreType.DMA((12,)),
+            pltpu.SemaphoreType.DMA((15,)),
             pltpu.SemaphoreType.DMA((packs, parts, 4)),
             pltpu.SemaphoreType.DMA((packs, 2, parts)),
-            pltpu.SemaphoreType.DMA((2, parts)),
-            pltpu.SemaphoreType.DMA((2, parts)),
+            pltpu.SemaphoreType.DMA((3, parts)),
+            pltpu.SemaphoreType.DMA((3, parts)),
             pltpu.SemaphoreType.DMA((row_tiles,)),
             pltpu.SemaphoreType.DMA((row_tiles,)),
+            pltpu.SemaphoreType.DMA((2, row_tiles)),
+            pltpu.SemaphoreType.DMA((2, row_tiles)),
+            pltpu.SemaphoreType.DMA((parts,)),
+            pltpu.SemaphoreType.DMA((parts,)),
+            pltpu.SemaphoreType.REGULAR,
         ],
         cost_estimate=pl.CostEstimate(
             flops=2 * length * model * (2 * channels + 2 * units) + 2 * length * model * (channels + units),

time: 246 us -> 218 us (0.89)
  the two profiles are of different devices: /device:TPU:0 before, /device:TPU:19 now
where the time goes in v2:
time: 218 us; the launch traced here: 217 us
  Pallas kernels  215 us (99%)
  local copies, waits for them, and re-layouts  2.3 us (1%)
    pallas_call x1, Pallas kernels, whole_layer(): pl.pallas_call(layer_kernel, in_specs=[hbm, hbm, hbm, vmem, hbm, hbm, vme...  215 us

profile of v2, /device:TPU:19, one launch (start us, length us, event | category | flops | bytes accessed | tf_op | source)
XLA Modules:
  0.0 217.4 jit_solution(13356609401306429223)
XLA Ops:
  0.0 215.1 %shard_map.136 = bf16[256,2048]{1,0:T(8,128)(2,1)} custom-call(bf16[512,2048]{1,0:T(8,128)(2,1)} %tok_hbm.1, bf16[256,1024]{1,0:T(8,128)(2,1)} %in_hbm.1, bf16[256,1024]{1,0:T(8,128)(2,1)} %gate_hbm.1, bf16[4,1024]{1,0:T(4,128)(2,1)} %taps_ref.1, bf16[4,256,256]{2,1,0:T(8,128)(2,1)} %rate_hbm.1, bf16[4,256,256]{2,1,0:T(8,128)(2,1)} %inlet_hbm.1, ...), custom_call_target="tpu_custom_call" | custom-call | flops 22548578304 | bytes 44040192 | tf_op jit(solution)/shard_map/pallas_call | solution.py:617
  215.1 2.3 %copy.16 = bf16[256,2048]{1,0:T(8,128)(2,1)} copy(bf16[256,2048]{1,0:T(8,128)(2,1)} %shard_map.136) | data formatting | bytes 2097152

commit v3 on v2

--- a/solution.py
+++ b/solution.py
@@ -82,40 +82,41 @@
 OWN, OWN_SIDE, FROM_SIDE, FROM_LINE, ON_SIDE, FROM_FAR_SIDE = range(6)
 A_PARTS = 1
 PACKS = ((0, 0, 1), (2, 0, 1), (3, 0, 1), (4, 0, 1), (5, 0, 2), (5, 1, 2), (6, 0, 1))
-ALONG = ((1, 1), (1, 1), (0, 0), (1, 1), (0, 0), (1, 1), (1, 1))
+ALONG = ((6, 7), (4, 5), (2, 3), (7, 6), (5, 5), (4, 5), (2, 2))
 PLANS = (
     (
-        (110, 331, 130, 10, 160, 421, 0, 402, 100, 200, 20, 403, 502, 531, 301, 522, 333, 210, 60, 311),
-        (501, 503, 302, 50, 431), (30, 230, 451, 412, 303), (413, 401), (513, 312, 512, 511, 120), (40,), (140,), (),
-        (), (341,), (), (332,), (441, 260, 313), (351,), (), (150,), (), (), (), (), (523, 461), (342,), (442, 453),
-        (), (), (452, 240), (553, 343, 541), (), (), (443, 321), (542,), (), (551,), (361, 352, 411), (), (), (533,),
-        (353,), (), (), (), (250, 323, 462, 552, 543), (220, 362), (), (363,), (), (), (562, 423, 532, 322), (433,),
-        (521, 463, 561), (), (563,), (), (), (422, 432),
+
+        (130, 220, 323, 0, 10, 100, 20, 332, 200, 401, 40, 402, 403, 303, 301, 501, 302, 502, 110, 503, 311, 150, 230, 411, 210, 412, 50, 413, 512, 313, 511, 60, 250),
+        (513, 312), (), (), (), (), (451, 433, 140, 30), (), (), (443, 160, 333), (), (), (), (461, 543, 551, 423),
+        (), (442,), (), (462,), (452,), (533,), (521,), (562,), (542, 343), (453, 260), (541, 523), (), (), (342,),
+        (), (), (361, 441), (), (), (331,), (), (531, 341, 353, 561, 240, 422), (), (351,), (), (532,),
+        (552, 553, 421, 362, 352), (), (463,), (), (432, 120, 363), (), (563,), (), (), (), (), (321, 431), (322,),
+        (), (522,),
     ),
     (
-
-        (522, 110, 100, 0, 130, 160, 60, 331, 333, 10, 50, 20, 210, 200, 531, 301, 402, 230, 30, 421, 40, 502, 501, 302, 401, 403, 451, 503, 413, 303, 311, 412, 120, 512, 313, 312, 513, 511, 361),
-        (260,), (), (), (140, 441), (523,), (), (442,), (), (341, 150), (), (), (), (453,), (), (), (452,),
-        (431, 332, 461), (), (323, 443), (), (), (411, 553, 240, 343, 352, 321, 250, 322, 541, 342), (), (), (), (),
-        (), (), (542,), (), (463,), (), (462, 351, 423, 533, 353), (), (521, 432, 551), (), (552,), (543,), (), (),
-        (362, 363), (), (), (), (532,), (), (), (433,), (), (), (), (422, 561, 563), (562,), (220,),
+        (130, 0, 323, 451, 10, 220, 110, 100, 200, 332, 402, 502, 20, 303, 301, 40, 230, 403, 210),
+        (503, 501, 411, 302, 311), (50, 413, 60, 313, 412, 150), (333,), (461,), (432, 160, 140), (),
+        (513, 533, 512, 511, 30), (), (), (250, 312), (), (), (523,), (), (423,), (443,), (433,), (462,), (441,), (),
+        (), (521,), (541, 442), (343, 452), (), (342,), (353, 453, 562), (), (240, 341, 361), (), (543, 561), (401,),
+        (532,), (551,), (), (531, 422), (), (351,), (), (542,), (553, 552), (), (), (352,), (463, 362, 522), (120,),
+        (), (363,), (), (), (), (260, 421), (431,), (322, 321, 563, 331),
     ),
     (
-        (140, 0, 150, 10, 311, 302, 301, 110, 100, 403, 303, 210, 200, 451, 20, 413, 402), (130, 501, 503),
-        (502, 511, 240, 312, 512, 313), (120, 40), (), (), (351,), (), (50,), (422, 421, 331, 513), (442,),
-        (342, 321, 401), (30,), (353,), (), (230, 341, 160), (60,), (433, 521, 531), (332,), (),
-        (423, 333, 250, 361, 352), (323, 523), (441, 533, 343, 453, 443, 522, 220, 532), (), (322, 362), (561,),
-        (542,), (541, 260), (), (), (), (), (), (363, 461, 463, 552), (), (), (), (), (), (431,), (562, 543), (), (),
-        (553, 551), (), (), (), (), (), (411,), (), (), (), (412,), (432, 452, 563, 462),
+
+        (0, 120, 100, 10, 412, 462, 302, 301, 403, 150, 200, 303, 311, 421, 503, 312, 110, 501, 341, 502, 313, 321, 441, 413, 60, 210),
+        (50, 511, 140, 40, 512, 513), (220, 362), (), (443, 323, 401), (531,), (452, 343), (20, 342), (352,), (422,),
+        (130, 423), (), (), (), (), (521, 551), (351, 442, 522), (552, 543), (402, 240, 411), (),
+        (322, 523, 331, 453, 250, 431, 353, 333, 230, 30, 160, 433), (332, 532, 533), (361,), (542,), (363, 553),
+        (461,), (541,), (432,), (), (), (), (), (463,), (260,), (), (563,), (562,), (), (), (), (), (561,), (), (),
+        (), (), (), (), (), (), (), (), (), (), (451,),
     ),
     (
-
-        (100, 130, 0, 302, 110, 150, 200, 301, 10, 120, 403, 502, 303, 311, 401, 413, 313, 501, 160, 60, 503, 511, 140, 441, 402, 210, 312, 321, 512, 451, 20),
-        (513, 40, 362), (), (50,), (), (422, 421, 351), (), (), (), (342, 442, 30), (353, 240), (), (220,),
-        (521, 352, 331), (), (332,), (531, 341, 423), (461,), (), (230, 522, 322, 323, 361, 433, 443, 523, 333),
-        (343, 533, 532, 250, 542, 453), (363,), (), (561, 553, 543, 541), (551, 552), (), (), (), (260,), (), (),
-        (463,), (431,), (), (), (), (563, 562), (), (), (), (), (), (), (411,), (), (), (), (), (412,), (), (), (),
-        (), (), (452, 462, 432),
+        (422, 441, 0, 110, 302, 100, 462, 120, 130, 301, 303, 311, 403, 200, 10, 501, 313),
+        (341, 502, 312, 413, 210, 412, 503, 150, 60, 50), (), (140, 421, 513), (), (), (220, 511), (443, 321),
+        (343,), (), (), (512,), (), (362, 452), (40,), (), (461, 240, 401, 20, 402), (521, 543, 531), (351, 342), (),
+        (423, 323, 331, 322, 552, 352), (551, 522, 250), (230, 353), (523, 411, 433, 442, 30), (361,), (160,), (),
+        (542,), (561,), (), (363,), (432, 532, 453, 533), (431, 332), (333,), (260,), (), (), (), (562,), (), (), (),
+        (553,), (), (463,), (), (541,), (), (), (), (), (), (), (), (563, 451),
     ),
 )
 
@@ -282,21 +283,22 @@
             for code in codes:
                 kind, pack, k = code // 100, code // 10 % 10, code % 10
                 first = PACKS[pack][0] in (3, 4)
-                along = ALONG[pack][second]
+                to_end, to_middle, from_end = (ALONG[pack][second] & bit for bit in (1, 2, 4))
                 if kind == OWN:
                     if not (first and in_middle):
                         send(pack, 0, 0, LINE, out)
                     if in_middle:
                         send(pack, 0, 0, OTHER, out)
                 elif kind == OWN_SIDE:
-                    if not first or in_middle or along:
+                    if not first or in_middle or from_end:
                         send(pack, 0, 0, SIDE, out)
                 elif kind == FROM_SIDE:
-                    if along:
-                        if not (first and in_middle):
-                            send(pack, 0, 1, LINE, out)
-                        if in_middle:
-                            send(pack, 0, 1, OTHER, out)
+                    if in_middle and to_end and not first:
+                        send(pack, 0, 1, LINE, out)
+                    if in_middle and to_middle:
+                        send(pack, 0, 1, OTHER, out)
+                    if not in_middle and from_end:
+                        send(pack, 0, 1, LINE, out)
                     if not first or in_middle:
                         send(pack, 0, 1, CORE, out)
                 elif first and not in_middle:
@@ -306,7 +308,8 @@
                         send(pack, k, 0, OTHER if k == 1 else LINE, out)
                     send(pack, k, 0, CORE, out)
                 elif kind == ON_SIDE:
-                    if k == 3 or not along or (k == 2 and not in_middle):
+                    comes_along = {1: from_end if in_middle else to_end, 2: in_middle and to_middle, 3: False}
+                    if not comes_along[k]:
                         send(pack, k, 0, SIDE, out)
                 else:
                     send(pack, k, 1, CORE, out)

time: 218 us -> 202 us (0.927)
  the two profiles are of different devices: /device:TPU:19 before, /device:TPU:20 now
where the time goes in v3:
time: 202 us
  Pallas kernels  200 us (99%)
  local copies, waits for them, and re-layouts  2.3 us (1%)
    pallas_call x1, Pallas kernels, whole_layer(): pl.pallas_call(layer_kernel, in_specs=[hbm, hbm, hbm, vmem, hbm, hbm, vme...  200 us

profile of v3, /device:TPU:20, one launch (start us, length us, event | category | flops | bytes accessed | tf_op | source)
XLA Modules:
  0.0 202.2 jit_solution(6320241203474500833)
XLA Ops:
  0.0 199.9 %shard_map.136 = bf16[256,2048]{1,0:T(8,128)(2,1)} custom-call(bf16[512,2048]{1,0:T(8,128)(2,1)} %tok_hbm.1, bf16[256,1024]{1,0:T(8,128)(2,1)} %in_hbm.1, bf16[256,1024]{1,0:T(8,128)(2,1)} %gate_hbm.1, bf16[4,1024]{1,0:T(4,128)(2,1)} %taps_ref.1, bf16[4,256,256]{2,1,0:T(8,128)(2,1)} %rate_hbm.1, bf16[4,256,256]{2,1,0:T(8,128)(2,1)} %inlet_hbm.1, ...), custom_call_target="tpu_custom_call" | custom-call | flops 22548578304 | bytes 44040192 | tf_op jit(solution)/shard_map/pallas_call | solution.py:620
  199.9 2.3 %copy.16 = bf16[256,2048]{1,0:T(8,128)(2,1)} copy(bf16[256,2048]{1,0:T(8,128)(2,1)} %shard_map.136) | data formatting | bytes 2097152

commit v4 on v3

--- a/solution.py
+++ b/solution.py
@@ -81,42 +81,42 @@
 INPUTS = 7
 OWN, OWN_SIDE, FROM_SIDE, FROM_LINE, ON_SIDE, FROM_FAR_SIDE = range(6)
 A_PARTS = 1
-PACKS = ((0, 0, 1), (2, 0, 1), (3, 0, 1), (4, 0, 1), (5, 0, 2), (5, 1, 2), (6, 0, 1))
-ALONG = ((6, 7), (4, 5), (2, 3), (7, 6), (5, 5), (4, 5), (2, 2))
+PACKS = ((0, 0, 1), (2, 0, 1), (3, 0, 1), (4, 0, 1), (5, 0, 1), (6, 0, 2), (6, 1, 2))
+ALONG = ((4, 5), (7, 7), (0, 1), (2, 3), (6, 7), (6, 3), (6, 3))
 PLANS = (
     (
 
-        (130, 220, 323, 0, 10, 100, 20, 332, 200, 401, 40, 402, 403, 303, 301, 501, 302, 502, 110, 503, 311, 150, 230, 411, 210, 412, 50, 413, 512, 313, 511, 60, 250),
-        (513, 312), (), (), (), (), (451, 433, 140, 30), (), (), (443, 160, 333), (), (), (), (461, 543, 551, 423),
-        (), (442,), (), (462,), (452,), (533,), (521,), (562,), (542, 343), (453, 260), (541, 523), (), (), (342,),
-        (), (), (361, 441), (), (), (331,), (), (531, 341, 353, 561, 240, 422), (), (351,), (), (532,),
-        (552, 553, 421, 362, 352), (), (463,), (), (432, 120, 363), (), (563,), (), (), (), (), (321, 431), (322,),
-        (), (522,),
+        (100, 0, 130, 110, 120, 301, 10, 200, 402, 433, 302, 210, 20, 30, 511, 401, 50, 403, 311, 501, 502, 503, 303, 423, 322, 40, 413),
+        (513, 412, 140, 323), (312, 313, 512), (160, 240), (), (), (), (), (), (), (533, 432, 332, 441), (), (),
+        (150,), (421,), (), (), (), (341, 342), (442, 541, 521), (), (351, 443, 343, 451), (532, 260), (), (),
+        (352,), (250,), (), (), (), (453, 542, 361, 461), (452, 60), (220, 462), (543, 353), (331,), (561,), (),
+        (531,), (333, 230), (), (), (562, 553), (), (463, 362), (), (), (431,), (552, 411, 551), (523, 363, 563), (),
+        (321,), (), (422,), (), (522,),
     ),
     (
-        (130, 0, 323, 451, 10, 220, 110, 100, 200, 332, 402, 502, 20, 303, 301, 40, 230, 403, 210),
-        (503, 501, 411, 302, 311), (50, 413, 60, 313, 412, 150), (333,), (461,), (432, 160, 140), (),
-        (513, 533, 512, 511, 30), (), (), (250, 312), (), (), (523,), (), (423,), (443,), (433,), (462,), (441,), (),
-        (), (521,), (541, 442), (343, 452), (), (342,), (353, 453, 562), (), (240, 341, 361), (), (543, 561), (401,),
-        (532,), (551,), (), (531, 422), (), (351,), (), (542,), (553, 552), (), (), (352,), (463, 362, 522), (120,),
-        (), (363,), (), (), (), (260, 421), (431,), (322, 321, 563, 331),
+        (10, 140, 120, 110, 100, 0, 20, 433, 210, 302, 402, 200, 30, 403, 502, 40, 301, 303, 501, 413, 503),
+        (240, 412, 50, 311, 423), (), (), (), (323, 401, 312, 130, 322), (512,), (), (511, 160, 313), (), (),
+        (533, 532, 432, 260, 332, 60, 513), (), (442,), (), (), (), (), (341, 521, 351, 150, 421), (), (), (),
+        (343,), (443, 543), (), (), (342,), (), (352, 441), (), (), (), (361,), (461, 542, 541, 451, 220), (462,),
+        (353, 452, 531, 331), (453,), (), (561,), (), (), (230, 333, 362), (), (463,), (), (411,), (), (),
+        (431, 553, 562), (552,), (), (551, 523), (), (563,), (321, 422, 363, 250, 522),
     ),
     (
 
-        (0, 120, 100, 10, 412, 462, 302, 301, 403, 150, 200, 303, 311, 421, 503, 312, 110, 501, 341, 502, 313, 321, 441, 413, 60, 210),
-        (50, 511, 140, 40, 512, 513), (220, 362), (), (443, 323, 401), (531,), (452, 343), (20, 342), (352,), (422,),
-        (130, 423), (), (), (), (), (521, 551), (351, 442, 522), (552, 543), (402, 240, 411), (),
-        (322, 523, 331, 453, 250, 431, 353, 333, 230, 30, 160, 433), (332, 532, 533), (361,), (542,), (363, 553),
-        (461,), (541,), (432,), (), (), (), (), (463,), (260,), (), (563,), (562,), (), (), (), (), (561,), (), (),
-        (), (), (), (), (), (), (), (), (), (), (451,),
+        (0, 110, 301, 302, 402, 311, 462, 100, 10, 210, 502, 403, 20, 130, 303, 501, 200, 413, 442, 503, 452, 512, 421, 120, 313, 513, 422, 511, 312, 331),
+        (), (), (), (), (322,), (522,), (), (140,), (), (220, 40, 321, 351, 341), (60,), (431, 432), (50, 240),
+        (423,), (), (353,), (412, 433, 333, 323), (541, 342), (), (343, 523, 521, 230, 533),
+        (443, 542, 401, 30, 352, 362, 332, 160, 531, 532), (543,), (461,), (361,), (), (453, 561), (150,),
+        (463, 363, 551), (), (), (), (), (), (260, 441, 250), (), (), (563, 553, 552, 562, 411), (), (), (), (), (),
+        (), (), (), (), (), (), (), (), (), (), (451,), (),
     ),
     (
-        (422, 441, 0, 110, 302, 100, 462, 120, 130, 301, 303, 311, 403, 200, 10, 501, 313),
-        (341, 502, 312, 413, 210, 412, 503, 150, 60, 50), (), (140, 421, 513), (), (), (220, 511), (443, 321),
-        (343,), (), (), (512,), (), (362, 452), (40,), (), (461, 240, 401, 20, 402), (521, 543, 531), (351, 342), (),
-        (423, 323, 331, 322, 552, 352), (551, 522, 250), (230, 353), (523, 411, 433, 442, 30), (361,), (160,), (),
-        (542,), (561,), (), (363,), (432, 532, 453, 533), (431, 332), (333,), (260,), (), (), (), (562,), (), (), (),
-        (553,), (), (463,), (), (541,), (), (), (), (), (), (), (), (563, 451),
+        (10, 0, 100, 110, 462, 130, 311, 402, 302, 301, 403, 313, 303, 442, 20, 200, 502, 413, 230, 312, 60),
+        (503, 513, 511, 331, 210, 40), (501, 431), (), (512, 321), (), (140,), (432, 532), (421,), (120, 342),
+        (341, 531), (), (422, 541), (50, 333), (362, 323), (), (), (343,), (412, 322, 401, 352, 522, 423, 433),
+        (523,), (), (361,), (160,), (443, 30, 220, 521), (351, 533, 240), (), (), (461,), (), (332,), (),
+        (260, 353, 150), (363,), (), (543,), (542,), (), (250,), (), (), (), (), (552,), (453,), (), (), (), (), (),
+        (451, 562, 441, 553), (463,), (), (411,), (), (452, 563, 551, 561),
     ),
 )
 
@@ -249,8 +249,8 @@
             count += 1
 
     steps = ["recur"] * blocks + ["mix"] * parts + ["terms"] + ["norm"] * row_tiles + ["rows"] * row_tiles
-    steps += ["first"] * first_tiles + ["far"] * parts + ["back"] * parts
-    steps += ["hidden"] * other_tiles + ["down"] * parts
+    steps += ["first"] * first_tiles + ["far"] * parts + ["hidden"] * other_tiles
+    steps += ["back"] * parts + ["down"] * parts
     begins = {name: steps.index(name) for name in dict.fromkeys(steps)}
     turn_of = [(0, 0), (0, 1), (1, 0), (2, 0), (1, 1), (3, 0), (2, 1), (3, 1)]
     needs = {begins["recur"]: 0, begins["mix"]: 2, begins["first"]: 3, begins["far"]: 4, begins["hidden"]: 5}
@@ -520,13 +520,18 @@
         )
 
     def back_step(s):
-        pl.when(s == 0)(lambda: terms_copy(2, parts - 1).start())
         terms_copy(2, s).wait_recv()
         came[0, s] = (terms[tp, s].astype(jnp.float32) + came[0, s].astype(jnp.float32)).astype(jnp.bfloat16)
         pl.when(s > 0)(lambda: back_copy(s - 1).start())
 
     loop("first", first_tiles, in_middle(first_step))
     loop("far", parts, in_middle(far_step))
+    def hidden_step(j):
+        to = pl.ds(pl.multiple_of(first_units + j * tile, tile), tile)
+        hidden[:, to] = units_at(normed, buf_c, j)
+        pl.when(jnp.logical_and(middle, j == 0))(lambda: terms_copy(2, parts - 1).start())
+
+    loop("hidden", other_tiles, hidden_step)
     loop("back", parts, in_middle(back_step))
 
     @pl.when(middle)
@@ -534,12 +539,6 @@
         for s in range(parts):
             terms_copy(2, s).wait_send()
         back_copy(parts - 1).start()
-
-    def hidden_step(j):
-        to = pl.ds(pl.multiple_of(first_units + j * tile, tile), tile)
-        hidden[:, to] = units_at(normed, buf_c, j)
-
-    loop("hidden", other_tiles, hidden_step)
 
     order = [spots[side][k] for k, side in turn_of]
 

time: 202 us -> 198 us (0.980)
  the two profiles are of different devices: /device:TPU:20 before, /device:TPU:0 now
where the time goes in v4:
time: 198 us; the launch traced here: 197 us
  Pallas kernels  194 us (98%)
  local copies, waits for them, and re-layouts  2.3 us (1%)
    pallas_call x1, Pallas kernels, whole_layer(): pl.pallas_call(layer_kernel, in_specs=[hbm, hbm, hbm, vmem, hbm, hbm, vme...  194 us

profile of v4, /device:TPU:0, one launch (start us, length us, event | category | flops | bytes accessed | tf_op | source)
XLA Modules:
  0.0 196.6 jit_solution(2089869459095406096)
XLA Ops:
  0.0 194.3 %shard_map.136 = bf16[256,2048]{1,0:T(8,128)(2,1)} custom-call(bf16[512,2048]{1,0:T(8,128)(2,1)} %tok_hbm.1, bf16[256,1024]{1,0:T(8,128)(2,1)} %in_hbm.1, bf16[256,1024]{1,0:T(8,128)(2,1)} %gate_hbm.1, bf16[4,1024]{1,0:T(4,128)(2,1)} %taps_ref.1, bf16[4,256,256]{2,1,0:T(8,128)(2,1)} %rate_hbm.1, bf16[4,256,256]{2,1,0:T(8,128)(2,1)} %inlet_hbm.1, ...), custom_call_target="tpu_custom_call" | custom-call | flops 22548578304 | bytes 44040192 | tf_op jit(solution)/shard_map/pallas_call | solution.py:619
  194.3 2.3 %copy.16 = bf16[256,2048]{1,0:T(8,128)(2,1)} copy(bf16[256,2048]{1,0:T(8,128)(2,1)} %shard_map.136) | data formatting | bytes 2097152

commit v5 on v4

--- a/solution.py
+++ b/solution.py
@@ -371,9 +371,12 @@
             gone.update(now)
             pl.when(mine)(functools.partial(act, [("sent", *one) for one in now]))
 
-    for group in loads:
-        for one in group:
-            one.start()
+    def begin(groups):
+        for group in groups:
+            for one in group:
+                one.start()
+
+    begin(loads[:A_PARTS])
     barrier = pltpu.get_barrier_semaphore()
     for target in [targets[LINE], targets[SIDE], targets[CORE], across]:
         pl.semaphore_signal(barrier, inc=1, device_id=target, device_id_type=MESH)
@@ -383,6 +386,7 @@
         pl.semaphore_signal(barrier, inc=1, device_id=targets[OTHER], device_id_type=MESH)
 
     pl.semaphore_wait(barrier, 4 + z * (3 - z) // 2)
+    begin(loads[A_PARTS:])
 
     def recur_step(i):
         cols = pl.ds(pl.multiple_of(i * block, block), block)
@@ -557,7 +561,7 @@
         pl.when(j > 0)(lambda: terms_copy(1, pick(j - 1)).start())
 
     loop("down", parts, down_step)
-    drain(range(5), len(steps))
+    drain(range(3), len(steps))
     terms_copy(1, order[-1]).start()
     drain(range(INPUTS), len(steps))
     for i in range(row_tiles):

time: 198 us -> 198 us (level)
  no operation moved by 1% of the time
where the time goes in v5:
time: 198 us; the launch traced here: 197 us
  Pallas kernels  194 us (98%)
  local copies, waits for them, and re-layouts  2.3 us (1%)
    pallas_call x1, Pallas kernels, whole_layer(): pl.pallas_call(layer_kernel, in_specs=[hbm, hbm, hbm, vmem, hbm, hbm, vme...  194 us

profile of v5, /device:TPU:0, one launch (start us, length us, event | category | flops | bytes accessed | tf_op | source)
XLA Modules:
  0.0 196.6 jit_solution(13307244748929730334)
XLA Ops:
  0.0 194.3 %shard_map.136 = bf16[256,2048]{1,0:T(8,128)(2,1)} custom-call(bf16[512,2048]{1,0:T(8,128)(2,1)} %tok_hbm.1, bf16[256,1024]{1,0:T(8,128)(2,1)} %in_hbm.1, bf16[256,1024]{1,0:T(8,128)(2,1)} %gate_hbm.1, bf16[4,1024]{1,0:T(4,128)(2,1)} %taps_ref.1, bf16[4,256,256]{2,1,0:T(8,128)(2,1)} %rate_hbm.1, bf16[4,256,256]{2,1,0:T(8,128)(2,1)} %inlet_hbm.1, ...), custom_call_target="tpu_custom_call" | custom-call | flops 22548578304 | bytes 44040192 | tf_op jit(solution)/shard_map/pallas_call | solution.py:623
  194.3 2.3 %copy.16 = bf16[256,2048]{1,0:T(8,128)(2,1)} copy(bf16[256,2048]{1,0:T(8,128)(2,1)} %shard_map.136) | data formatting | bytes 2097152
